TPU v7x, 32 devices: a whole 2x2x4 slice. The times are simulated.
32 devices in a mesh: sp: 8 (over z, x), tp: 4 (over y, core).
Axes of the slice: x: 2, y: 2, z: 4, core: 2. Of those that a mesh axis runs over, the one named last changes fastest.
Arguments:
- target: bfloat16 [1024, 4096], P('sp', 'tp'), may hold values from -300 to 300
- gain: float32 [4096], P('tp'), may hold values from 0.1 to 1.9
- w_query: bfloat16 [4096, 4096], P('tp'), may hold values from -0.09375 to 0.09375
- queries: bfloat16 [1024, 4096], P('sp', 'tp'), may hold values from -13 to 13
- keys: bfloat16 [4096, 1024], P('sp'), may hold values from -4 to 4
- values: bfloat16 [4096, 1024], P('sp'), may hold values from -4 to 4
- attn_out: bfloat16 [1024, 4096], P('sp', 'tp'), may hold values from -4 to 4
- grad_out: bfloat16 [1024, 4096], P('sp', 'tp'), may hold values from -64 to 64
Outputs:
- grad_rows: bfloat16 [1024, 4096], P('sp', 'tp')
- grad_weight: float32 [4096, 4096], P(('tp', 'sp'))
- grad_keys: float32 [4096, 1024], P(('sp', 'tp'))
- grad_values: float32 [4096, 1024], P(('sp', 'tp'))
All inputs are finite; a program needn't handle non-finite values.
Results may differ from a plain program's by a relative error of at most 0.018.
Values may be sent and summed in bfloat16 or wider, within the bound.
A program may use at most 64 MiB of HBM per device.

v0:
```python
import functools
import math

import jax
import jax.numpy as jnp
from jax import lax
from jax.experimental import pallas as pl
from jax.experimental.pallas import tpu as pltpu
from jax.sharding import PartitionSpec as P

WIDTH = 4096
HEADS = 16
KV_HEADS = 4
HEAD_DIM = 256


norm_eps = 1e-06


def merged(part, axis, combine):
    gathered = jax.tree.map(lambda a: lax.all_gather(a, axis), part)

    def take(source):
        return jax.tree.map(lambda a: lax.dynamic_index_in_dim(a, source, 0, False), gathered)

    return lax.fori_loop(
        1, lax.axis_size(axis), lambda source, state: combine(state, take(source)), take(0)
    )


def join_stats(first_part, second_part):
    row_peak = jnp.maximum(first_part[0], second_part[0])
    summed = first_part[1] * jnp.exp(first_part[0] - row_peak) + second_part[1] * jnp.exp(
        second_part[0] - row_peak
    )
    return (row_peak, summed, first_part[2] + second_part[2])


def local(target, gain, w_query, queries, keys, values, attn_out, grad_out):
    local_heads = queries.shape[1] // HEAD_DIM
    group_size = HEADS // KV_HEADS
    score_scale = HEAD_DIM ** (-0.5)
    own_rows = queries.shape[0]
    src_rows = keys.shape[0]
    kv_index = lax.axis_index("tp") * local_heads // group_size
    key_own = lax.dynamic_slice_in_dim(keys, kv_index * HEAD_DIM, HEAD_DIM, 1)
    value_own = lax.dynamic_slice_in_dim(values, kv_index * HEAD_DIM, HEAD_DIM, 1)
    out_heads = attn_out.reshape(own_rows, local_heads, HEAD_DIM).astype(jnp.float32)
    grad_heads = grad_out.reshape(own_rows, local_heads, HEAD_DIM).astype(jnp.float32)
    delta_own = jnp.sum(out_heads * grad_heads, axis=2)
    empty_sum = jnp.zeros((src_rows, HEAD_DIM), jnp.float32)
    total_rows = own_rows * lax.axis_size("sp")
    position = lax.axis_index("sp") * own_rows
    delta_full = lax.dynamic_update_slice_in_dim(
        jnp.zeros((total_rows, local_heads), jnp.float32), delta_own, position, 0
    )
    query_all, grad_all = (
        lax.all_gather(queries, "sp", axis=0, tiled=True),
        lax.all_gather(grad_out, "sp", axis=0, tiled=True),
    )
    block_rows = math.gcd(total_rows, 512)
    block_count = total_rows // block_rows
    query_blocks = query_all.reshape(block_count, block_rows, local_heads, HEAD_DIM)
    grad_blocks = grad_all.reshape(block_count, block_rows, local_heads, HEAD_DIM)

    def block_stats(query_block):
        scores = (
            jnp.einsum("qhd,sd->hqs", query_block, key_own, preferred_element_type=jnp.float32)
            * score_scale
        )
        row_peak = jnp.max(scores, axis=2)
        row_total = jnp.sum(jnp.exp(scores - row_peak[:, :, None]), axis=2)
        return (row_peak, row_total)

    peaks, totals = lax.map(block_stats, query_blocks)
    peaks, totals, delta_full = merged((peaks, totals, delta_full), "sp", join_stats)
    log_totals = peaks + jnp.log(totals)
    delta_blocks = delta_full.reshape(block_count, block_rows, local_heads)

    def block_grads(running, inputs):
        query_block, grad_block, delta_block, log_block = inputs
        scores = (
            jnp.einsum("qhd,sd->hqs", query_block, key_own, preferred_element_type=jnp.float32)
            * score_scale
        )
        weights = jnp.exp(scores - log_block[:, :, None])
        grad_weights = jnp.einsum(
            "qhd,sd->hqs", grad_block, value_own, preferred_element_type=jnp.float32
        )
        delta_cols = jnp.transpose(delta_block)
        grad_scores = (weights * (grad_weights - delta_cols[:, :, None]) * score_scale).astype(
            jnp.bfloat16
        )
        key_sum = running[0] + jnp.einsum(
            "hqs,qhd->sd", grad_scores, query_block, preferred_element_type=jnp.float32
        )
        value_sum = running[1] + jnp.einsum(
            "hqs,qhd->sd",
            weights.astype(jnp.bfloat16),
            grad_block,
            preferred_element_type=jnp.float32,
        )
        query_part = jnp.einsum(
            "hqs,sd->qhd", grad_scores, key_own, preferred_element_type=jnp.float32
        )
        return ((key_sum, value_sum), query_part)

    (key_sum, value_sum), query_parts = lax.scan(
        block_grads, (empty_sum, empty_sum), (query_blocks, grad_blocks, delta_blocks, log_totals)
    )
    query_parts = query_parts.reshape(total_rows, 1, local_heads * HEAD_DIM)
    received = lax.all_to_all(
        query_parts.astype(jnp.bfloat16), "sp", split_axis=0, concat_axis=1, tiled=True
    ).astype(query_parts.dtype)
    query_grad = jnp.sum(received, axis=1)
    key_cols = key_sum.reshape(src_rows, 1, HEAD_DIM)
    value_cols = value_sum.reshape(src_rows, 1, HEAD_DIM)
    key_parts, value_parts = (
        lax.all_to_all(
            key_cols.astype(jnp.bfloat16), "tp", split_axis=0, concat_axis=1, tiled=True
        ).astype(key_cols.dtype),
        lax.all_to_all(
            value_cols.astype(jnp.bfloat16), "tp", split_axis=0, concat_axis=1, tiled=True
        ).astype(value_cols.dtype),
    )
    part_rows = key_parts.shape[0]
    per_kv = key_parts.shape[1] // KV_HEADS
    grad_keys = (
        key_parts.reshape(part_rows, KV_HEADS, per_kv, HEAD_DIM)
        .sum(axis=2)
        .reshape(part_rows, KV_HEADS * HEAD_DIM)
    )
    grad_values = (
        value_parts.reshape(part_rows, KV_HEADS, per_kv, HEAD_DIM)
        .sum(axis=2)
        .reshape(part_rows, KV_HEADS * HEAD_DIM)
    )
    query_grad = query_grad.astype(jnp.bfloat16)
    query_all_heads = lax.all_gather(query_grad, "tp", axis=1, tiled=True)
    grad_rows = lax.dot_general(
        query_all_heads, w_query, (((1,), (1,)), ((), ())), preferred_element_type=jnp.float32
    ).astype(jnp.bfloat16)
    target_wide = target.astype(jnp.float32)
    squares = lax.psum(jnp.sum(target_wide * target_wide, axis=1), "tp")
    inverse = lax.rsqrt(squares / WIDTH + norm_eps)
    normed = (target_wide * inverse[:, None] * gain).astype(jnp.bfloat16)
    grad_weight = lax.psum_scatter(
        lax.dot_general(
            normed, query_all_heads, (((0,), (0,)), ((), ())), preferred_element_type=jnp.float32
        ).astype(jnp.bfloat16),
        "sp",
        scatter_dimension=0,
        tiled=True,
    ).astype(jnp.float32)
    return (grad_rows, grad_weight, grad_keys, grad_values)


MESH = pl.DeviceIdType.MESH
BF16, F32 = jnp.bfloat16, jnp.float32
NT = (((1,), (1,)), ((), ()))
X = 2
CHUNK = 256


def fused_kernel(
    zs, ts, heads,
    target, gain, w_query, queries, keys, values, attn_out, grad_out,
    grad_rows, grad_weight, grad_keys, grad_values,
    qs, dos, outs, kbuf, vbuf, ktr, delta, sbuf, pbuf, dsbuf, qpart, qpart_in,
    stat, stat_in, ksum, kv_out, kv_in, kv_tp, kv_tp_in, sq, ntr, nall,
    qown, qg, qt, wbuf, res_out, res_in, send, recv, local_sem, zsend, zrecv, psend, precv, qxs, qxr,
):
    rows = queries.shape[0]
    src = keys.shape[0]
    hd = HEAD_DIM
    width = heads * hd
    cols = heads * rows
    part = src // ts
    feat = target.shape[1] // (zs * X)
    scale = hd ** (-0.5)
    sp, tp = lax.axis_index("sp"), lax.axis_index("tp")
    z, x = sp // X, sp % X
    counter = [0]
    pending = []

    def zpeer(d, dx=0):
        return (((z + d) % zs) * X + (x + dx) % X, tp)

    def tpeer(e):
        return (sp, (tp + e) % ts)

    def push(source, dest, device):
        i = counter[0]
        counter[0] += 1
        copy = pltpu.make_async_remote_copy(
            src_ref=source, dst_ref=dest, send_sem=send.at[i], recv_sem=recv.at[i],
            device_id=device, device_id_type=MESH,
        )
        copy.start()
        pending.append(copy)
        return copy

    def run(device, source, dest, ssem, rsem):
        return pltpu.make_async_remote_copy(
            src_ref=source, dst_ref=dest, send_sem=ssem, recv_sem=rsem,
            device_id=device, device_id_type=MESH,
        )

    first = (zs - 1 - z) // (zs - 1)
    last = z // (zs - 1)
    inner = first + last == 0
    near = [1 + 2 * first, 3 - first - last, 2 - first + last]

    def hops(stream, view, d):
        up = run(
            zpeer(1), view(d), view((d + 1) % zs), zsend.at[stream, d, 0],
            zrecv.at[stream, (d + 1) % zs],
        )
        down = run(
            zpeer(zs - 1), view(d), view((d + zs - 1) % zs), zsend.at[stream, d, 1],
            zrecv.at[stream, (d + zs - 1) % zs],
        )
        below, above = z >= d, z < d
        if isinstance(d, int) and d == 0:
            above = z >= 0
        return ((up, below & (z < zs - 1)), (down, above & (z > 0)))

    def forward(stream, view, d):
        for copy, wanted in hops(stream, view, d):
            pl.when(wanted)(copy.start)

    def arrived(stream, view, d):
        run(zpeer(1), view(0), view(d), zsend.at[stream, 0, 0], zrecv.at[stream, d]).wait_recv()

    def relay(stream, view, d):
        arrived(stream, view, d)
        forward(stream, view, d)

    q_view, d_view = (lambda d: qs.at[d]), (lambda d: dos.at[d])
    half = width // 2

    def g_view(b, dx=0):
        return lambda d: qg.at[b, pl.ds(pl.multiple_of((d * X + dx) * rows, rows), rows)]

    streams = ((0, q_view), (1, d_view), (2, g_view(0)), (3, g_view(1)))

    local_count = [0]

    def fetch(source, dest):
        i = local_count[0]
        local_count[0] += 1
        copy = pltpu.make_async_copy(source, dest, local_sem.at[i])
        copy.start()
        return copy

    head_col = pl.ds(pl.multiple_of(tp * hd, hd), hd)
    q_loads, d_loads, o_loads = [], [], []
    kv_loads = [
        fetch(keys.at[:, head_col], kbuf.at[pl.ds(0, src)]),
        fetch(values.at[:, head_col], vbuf.at[pl.ds(0, src)]),
    ]
    for ref, buf, loads in ((queries, qs, q_loads), (grad_out, dos, d_loads), (attn_out, outs, o_loads)):
        for h in range(heads):
            view = buf.at[pl.ds(h * rows, rows)] if buf is outs else buf.at[0, pl.ds(h * rows, rows)]
            loads.append(fetch(ref.at[:, pl.ds(h * hd, hd)], view))
    w_loads = []
    for e in range(ts):
        w_col = pl.ds(pl.multiple_of(((tp + ts - e) % ts) * width, width), width)
        w_loads.append(fetch(w_query.at[:, w_col], wbuf.at[e]))

    barrier = pltpu.get_barrier_semaphore()
    peers = [zpeer(d, dx) for d in range(zs) for dx in range(X) if d + dx]
    peers += [tpeer(e) for e in range(1, ts)]
    for peer in peers:
        pl.semaphore_signal(barrier, inc=1, device_id=peer, device_id_type=MESH)
    pl.semaphore_wait(barrier, len(peers))

    order = [1, zs - 1] + list(range(2, zs - 1)) if zs > 2 else list(range(1, zs))
    for copy in q_loads:
        copy.wait()
    forward(0, q_view, 0)
    for copy in kv_loads:
        copy.wait()
    k_in = push(kbuf.at[pl.ds(0, src)], kbuf.at[pl.ds(src, src)], zpeer(0, 1))
    v_in = push(vbuf.at[pl.ds(0, src)], vbuf.at[pl.ds(src, src)], zpeer(0, 1))
    for copy in d_loads:
        copy.wait()
    forward(1, d_view, 0)

    wide = target[...].astype(F32)
    sq[0] = jnp.broadcast_to(jnp.sum(wide * wide, axis=1, keepdims=True), (rows, 128))
    sq_in = [push(sq.at[0], sq.at[e], tpeer(e)) for e in range(1, ts)]

    for copy in o_loads:
        copy.wait()
    for h in range(heads):
        span = pl.ds(h * rows, rows)
        dot = jnp.sum(dos[0, span].astype(F32) * outs[span].astype(F32), axis=1, keepdims=True)
        delta[0, :, span] = jnp.broadcast_to(dot, (rows, 128)).T[:8]
    delta_in = {d: push(delta.at[0], delta.at[d], zpeer(d)) for d in order}

    for copy in sq_in:
        copy.wait_recv()
    total = sq[0]
    for e in range(1, ts):
        total = total + sq[e]
    inverse = lax.rsqrt(total[:, :1] / (target.shape[1] * ts) + norm_eps)
    normed = target[...].astype(F32) * inverse * gain[...]
    ntr[...] = normed.T.astype(BF16)

    def feature_rows(d, dx):
        owner = ((z + d) % zs) * X + (x + dx) % X
        return pl.ds(pl.multiple_of(owner * feat, feat), feat)

    n_in = []
    for d in range(zs):
        for dx in range(X):
            lanes = pl.ds((d * X + dx) * rows, rows)
            if d + dx:
                n_in.append(
                    push(ntr.at[feature_rows(d, dx)], nall.at[0, :, lanes], zpeer(d, dx))
                )
            else:
                nall[0, :, lanes] = ntr[feature_rows(0, 0)]

    chunks = X * src // CHUNK

    def scores_of(d):
        def step(c, peak):
            span = pl.ds(pl.multiple_of(c * CHUNK, CHUNK), CHUNK)
            s = lax.dot_general(kbuf[span], qs[d], NT, preferred_element_type=F32)
            sbuf[span] = s
            return jnp.maximum(peak, jnp.max(s, axis=0, keepdims=True))

        return lax.fori_loop(0, chunks, step, jnp.full((1, cols), -jnp.inf, F32))

    def grads_of(d, peak):
        own_delta = delta[d, :1]

        def step(c, total):
            span = pl.ds(pl.multiple_of(c * CHUNK, CHUNK), CHUNK)
            p = jnp.exp((sbuf[span] - peak) * scale)
            dp = lax.dot_general(vbuf[span], dos[d], NT, preferred_element_type=F32)
            pbuf[d, span] = p.astype(BF16)
            dsbuf[d, span] = (p * (dp - own_delta) * scale).astype(BF16)
            return total + jnp.sum(p, axis=0, keepdims=True)

        total = lax.fori_loop(0, chunks, step, jnp.zeros((1, cols), F32))
        stat[d, 0:1] = peak * scale
        stat[d, 1:2] = total
        stat[d, 2:8] = jnp.zeros((6, cols), F32)
        return jnp.dot(ktr[...], dsbuf[d], preferred_element_type=F32)

    def process(d):
        peak = scores_of(d)
        qpart[d] = grads_of(d, peak).astype(BF16)

    def part_copy(d):
        return run(zpeer(zs - d), qpart.at[d], qpart_in.at[d], psend.at[d], precv.at[d])

    relay(0, q_view, near[0])
    ktr[:, :src] = kbuf[:src].T
    k_in.wait_recv()
    ktr[:, src:] = kbuf[src:].T
    relay(1, d_view, near[0])
    v_in.wait_recv()

    @pl.when(inner)
    def _():
        relay(0, q_view, near[1])
        relay(1, d_view, near[1])

    for copy in delta_in.values():
        copy.wait_recv()
    process(0)

    @pl.when(inner)
    def _():
        relay(0, q_view, near[2])

    process(near[0])
    part_copy(near[0]).start()

    @pl.when(inner)
    def _():
        relay(1, d_view, near[2])

    @pl.when(first + last > 0)
    def _():
        arrived(0, q_view, near[1])
        arrived(1, d_view, near[1])

    process(near[1])
    part_copy(near[1]).start()

    @pl.when(first + last > 0)
    def _():
        arrived(0, q_view, near[2])
        arrived(1, d_view, near[2])

    process(near[2])
    part_copy(near[2]).start()
    for copy in n_in:
        copy.wait_recv()
    nt_in = [push(nall.at[0], nall.at[e], tpeer(e)) for e in range(1, ts)]

    stat_copies = [push(stat, stat_in.at[d], zpeer(d)) for d in order]
    for copy in stat_copies:
        copy.wait_recv()

    def stats_of(d, e):
        ref = stat.at[d] if e == 0 else stat_in.at[e, (d + zs - e) % zs]
        return ref[0:1], ref[1:2]

    def ratios(d):
        parts = [stats_of(d, e) for e in range(zs)]
        top = parts[0][0]
        for m, _ in parts[1:]:
            top = jnp.maximum(top, m)
        factors = [jnp.exp(m - top) for m, _ in parts]
        summed = sum(f * l for f, (_, l) in zip(factors, parts))
        return [f / summed for f in factors]

    own_ratios = ratios(0)
    for d in range(zs):
        r = own_ratios[0] if d == 0 else ratios(d)[0]
        r = jnp.broadcast_to(r, (128, cols)).T
        r = jnp.concatenate([r] * (hd // 128), axis=1)
        sbuf_q = (qs[d].astype(F32) * r).astype(BF16)
        sbuf_d = (dos[d].astype(F32) * r).astype(BF16)
        for i, (left, right) in enumerate(((dsbuf, sbuf_q), (pbuf, sbuf_d))):
            piece = jnp.dot(left[d], right, preferred_element_type=F32)
            ksum[i] = piece if d == 0 else ksum[i] + piece
    kv_out[...] = ksum[:, src:].astype(BF16)
    kvx_in = push(kv_out, kv_in, zpeer(0, 1))

    grad_t = qpart[0].astype(F32) * own_ratios[0]
    for d in order:
        part_copy(d).wait_recv()
        grad_t = grad_t + qpart_in[d].astype(F32) * own_ratios[(zs - d) % zs]
    grad_own = grad_t.T
    for h in range(heads):
        piece = grad_own[h * rows : (h + 1) * rows].astype(BF16)
        qown[:, pl.ds(h * hd, hd)] = piece
        b, at = h * hd // half, h * hd % half
        qg[b, pl.ds(0, rows), pl.ds(at, hd)] = piece
    def cross(b, d):
        run(zpeer(0, 1), g_view(b)(d), g_view(b, 1)(d), qxs.at[b, d], qxr.at[b, d]).start()

    forward(2, g_view(0), 0)
    cross(0, 0)
    qt_in = {e: push(qown, qt.at[e], tpeer(e)) for e in range(1, ts)}
    relay(2, g_view(0), near[0])
    forward(3, g_view(1), 0)
    cross(0, near[0])
    cross(1, 0)

    kvx_in.wait_recv()
    for i in range(2):
        ksum[i, :src] = ksum[i, :src] + kv_in[i].astype(F32)
    kv_tp[...] = ksum[:, :src].astype(BF16)

    def part_rows(e):
        return pl.ds(pl.multiple_of(((tp + e) % ts) * part, part), part)

    kvt_in = [push(kv_tp.at[:, part_rows(e)], kv_tp_in.at[e], tpeer(e)) for e in range(1, ts)]
    for i, out in enumerate((grad_keys, grad_values)):
        out[:, head_col] = ksum[i, part_rows(0)]

    w_loads[0].wait()
    rows_sum = lax.dot_general(qown[...], wbuf[0], NT, preferred_element_type=F32)
    relay(2, g_view(0), near[1])
    cross(0, near[1])
    relay(3, g_view(1), near[0])
    cross(1, near[0])
    relay(2, g_view(0), near[2])
    cross(0, near[2])
    relay(3, g_view(1), near[1])
    cross(1, near[1])
    for e in range(1, ts):
        kvt_in[e - 1].wait_recv()
        at = pl.ds(pl.multiple_of(((tp + ts - e) % ts) * hd, hd), hd)
        for i, out in enumerate((grad_keys, grad_values)):
            out[:, at] = kv_tp_in[e, i].astype(F32)
    for copy in nt_in:
        copy.wait_recv()
    def crossed(b):
        for d in range(zs):
            run(zpeer(0, 1), g_view(b)(d), g_view(b, 1)(d), qxs.at[b, d], qxr.at[b, d]).wait_recv()

    res_copies = {}

    def project(b):
        for e in [*range(1, ts), 0]:
            piece = jnp.dot(nall[e], qg[b], preferred_element_type=F32)
            if e:
                res_out[b, e] = piece.astype(BF16)
                res_copies[b, e] = push(res_out.at[b, e], res_in.at[b, e], tpeer(ts - e))
            else:
                grad_weight[:, pl.ds(pl.multiple_of(tp * width + b * half, half), half)] = piece

    crossed(0)
    project(0)
    relay(3, g_view(1), near[2])
    cross(1, near[2])
    for e in range(1, ts):
        qt_in[e].wait_recv()
        w_loads[e].wait()
        rows_sum = rows_sum + lax.dot_general(qt[e], wbuf[e], NT, preferred_element_type=F32)
    grad_rows[...] = rows_sum.astype(BF16)
    crossed(1)
    project(1)
    for b in range(2):
        for e in range(1, ts):
            res_copies[b, e].wait_recv()
            at = ((tp + e) % ts) * width + b * half
            grad_weight[:, pl.ds(pl.multiple_of(at, half), half)] = res_in[b, e].astype(F32)
    for stream, view in streams:
        for d in range(zs):
            for copy, wanted in hops(stream, view, d):
                pl.when(wanted)(copy.wait_send)
    for d in range(1, zs):
        part_copy(d).wait_send()
    for b in range(2):
        for d in range(zs):
            run(zpeer(0, 1), g_view(b)(d), g_view(b, 1)(d), qxs.at[b, d], qxr.at[b, d]).wait_send()
    for copy in pending:
        copy.wait_send()


def fused(target, gain, w_query, queries, keys, values, attn_out, grad_out):
    zs, ts = lax.axis_size("sp") // X, lax.axis_size("tp")
    rows, width = queries.shape
    src = keys.shape[0]
    heads = width // HEAD_DIM
    cols, hd = heads * rows, HEAD_DIM
    feats = target.shape[1]
    feat = feats // (zs * X)
    part = src // ts
    copies = 6 * zs * X + 8 * ts + 16
    vmem, hbm = pl.BlockSpec(memory_space=pltpu.VMEM), pl.BlockSpec(memory_space=pl.ANY)
    return pl.pallas_call(
        functools.partial(fused_kernel, zs, ts, heads),
        out_shape=(
            jax.ShapeDtypeStruct((rows, feats), BF16),
            jax.ShapeDtypeStruct((feat, width * ts), F32),
            jax.ShapeDtypeStruct((part, keys.shape[1]), F32),
            jax.ShapeDtypeStruct((part, keys.shape[1]), F32),
        ),
        in_specs=[vmem, vmem, hbm, hbm, hbm, hbm, hbm, hbm],
        out_specs=(vmem,) * 4,
        scratch_shapes=[
            pltpu.VMEM((zs, cols, hd), BF16),
            pltpu.VMEM((zs, cols, hd), BF16),
            pltpu.VMEM((cols, hd), BF16),
            pltpu.VMEM((X * src, hd), BF16),
            pltpu.VMEM((X * src, hd), BF16),
            pltpu.VMEM((hd, X * src), BF16),
            pltpu.VMEM((zs, 8, cols), F32),
            pltpu.VMEM((X * src, cols), F32),
            pltpu.VMEM((zs, X * src, cols), BF16),
            pltpu.VMEM((zs, X * src, cols), BF16),
            pltpu.VMEM((zs, hd, cols), BF16),
            pltpu.VMEM((zs, hd, cols), BF16),
            pltpu.VMEM((zs, 8, cols), F32),
            pltpu.VMEM((zs, zs, 8, cols), F32),
            pltpu.VMEM((2, X * src, hd), F32),
            pltpu.VMEM((2, src, hd), BF16),
            pltpu.VMEM((2, src, hd), BF16),
            pltpu.VMEM((2, src, hd), BF16),
            pltpu.VMEM((ts, 2, part, hd), BF16),
            pltpu.VMEM((ts, rows, 128), F32),
            pltpu.VMEM((feats, rows), BF16),
            pltpu.VMEM((ts, feat, zs * X * rows), BF16),
            pltpu.VMEM((rows, width), BF16),
            pltpu.VMEM((2, zs * X * rows, width // 2), BF16),
            pltpu.VMEM((ts, rows, width), BF16),
            pltpu.VMEM((ts, feats, width), BF16),
            pltpu.VMEM((2, ts, feat, width // 2), BF16),
            pltpu.VMEM((2, ts, feat, width // 2), BF16),
            pltpu.SemaphoreType.DMA((copies,)),
            pltpu.SemaphoreType.DMA((copies,)),
            pltpu.SemaphoreType.DMA((2 + 3 * heads + ts,)),
            pltpu.SemaphoreType.DMA((4, zs, 2)),
            pltpu.SemaphoreType.DMA((4, zs)),
            pltpu.SemaphoreType.DMA((zs,)),
            pltpu.SemaphoreType.DMA((zs,)),
            pltpu.SemaphoreType.DMA((2, zs)),
            pltpu.SemaphoreType.DMA((2, zs)),
        ],
        compiler_params=pltpu.CompilerParams(
            collective_id=0, has_side_effects=True, vmem_limit_bytes=60 * 2**20
        ),
    )(target, gain.reshape(1, feats), w_query, queries, keys, values, attn_out, grad_out)


def fits(mesh):
    sp, tp = mesh.shape["sp"], mesh.shape["tp"]
    feat = WIDTH // (sp * tp)
    return tp == KV_HEADS and sp == 4 * X and feat % 128 == 0


def solution(mesh):
    return jax.shard_map(
        fused if fits(mesh) else local,
        mesh=mesh,
        in_specs=(
            P("sp", "tp"),
            P("tp"),
            P("tp", None),
            P("sp", "tp"),
            P("sp", None),
            P("sp", None),
            P("sp", "tp"),
            P("sp", "tp"),
        ),
        out_specs=(
            P("sp", "tp"),
            P(("tp", "sp"), None),
            P(("sp", "tp"), None),
            P(("sp", "tp"), None),
        ),
        check_vma=False,
    )
```

profile of v0, /device:TPU:1, one launch (start us, length us, event | category | flops | bytes accessed | tf_op | source)
XLA Modules:
  0.0 133.3 jit_solution(2351432008982683415)
XLA Ops:
  0.6 126.1 %shard_map.111 = (bf16[128,1024]{1,0:T(8,128)(2,1)}, f32[128,4096]{1,0:T(8,128)}, f32[128,1024]{1,0:T(8,128)}, f32[128,1024]{1,0:T(8,128)}) custom-call(bf16[128,1024]{1,0:T(8,128)(2,1)} %target.1, f32[1,1024]{1,0:T(1,128)} %bitcast.1, bf16[1024,4096]{1,0:T(8,128)(2,1)} %w_query.1, bf16[128,1024]{1,0:T(8,128)(2,1)} %queries.1, bf16[512,1024]{1,0:T(8,128)(2,1)} %keys.1, ...), custom_call_target="tpu_custom_call" | custom-call | tf_op jit(solution)/shard_map/pallas_call | solution.py:542
  126.8 1.7 %copy.16 = bf16[128,1024]{1,0:T(8,128)(2,1)} copy(bf16[128,1024]{1,0:T(8,128)(2,1)} %get-tuple-element.8) | data formatting | bytes 524288
  128.5 0.0 copy-start.1
  128.5 0.0 copy-start
  128.5 3.2 %copy.17 = f32[128,4096]{1,0:T(8,128)} copy(f32[128,4096]{1,0:T(8,128)} %get-tuple-element.9) | data formatting | bytes 4194304
  131.7 0.0 copy-done.1
  131.7 0.8 copy.18
  132.5 0.0 copy-done
  132.5 0.8 copy.19
Async XLA Ops:
  128.5 3.2 %copy-start.1 = (f32[128,1024]{1,0:T(8,128)S(1)}, f32[128,1024]{1,0:T(8,128)}, u32[]{:S(2)}) copy-start(f32[128,1024]{1,0:T(8,128)} %get-tuple-element.10) | copy-start | bytes 1572868
  128.5 4.0 %copy-start = (f32[128,1024]{1,0:T(8,128)S(1)}, f32[128,1024]{1,0:T(8,128)}, u32[]{:S(2)}) copy-start(f32[128,1024]{1,0:T(8,128)} %get-tuple-element.11) | copy-start | bytes 1572868
where the time goes:
time: 136 us; the launch traced here: 133 us
  Pallas kernels  126 us (93%)
  local copies, waits for them, and re-layouts  6.46 us (5%)
    pallas_call x1, Pallas kernels, fused(): pl.pallas_call(functools.partial(fused_kernel, zs, ts, heads), out_shape=...  126 us
    unnamed x8, local copies, waits for them, and re-layouts  6.46 us

commit v1 on v0

v1 whole, which is shorter than its diff:
```python
import functools
import math

import jax
import jax.numpy as jnp
from jax import lax
from jax.experimental import pallas as pl
from jax.experimental.pallas import tpu as pltpu
from jax.sharding import PartitionSpec as P

WIDTH = 4096
HEADS = 16
KV_HEADS = 4
HEAD_DIM = 256


norm_eps = 1e-06


def merged(part, axis, combine):
    gathered = jax.tree.map(lambda a: lax.all_gather(a, axis), part)

    def take(source):
        return jax.tree.map(lambda a: lax.dynamic_index_in_dim(a, source, 0, False), gathered)

    return lax.fori_loop(
        1, lax.axis_size(axis), lambda source, state: combine(state, take(source)), take(0)
    )


def join_stats(first_part, second_part):
    row_peak = jnp.maximum(first_part[0], second_part[0])
    summed = first_part[1] * jnp.exp(first_part[0] - row_peak) + second_part[1] * jnp.exp(
        second_part[0] - row_peak
    )
    return (row_peak, summed, first_part[2] + second_part[2])


def local(target, gain, w_query, queries, keys, values, attn_out, grad_out):
    local_heads = queries.shape[1] // HEAD_DIM
    group_size = HEADS // KV_HEADS
    score_scale = HEAD_DIM ** (-0.5)
    own_rows = queries.shape[0]
    src_rows = keys.shape[0]
    kv_index = lax.axis_index("tp") * local_heads // group_size
    key_own = lax.dynamic_slice_in_dim(keys, kv_index * HEAD_DIM, HEAD_DIM, 1)
    value_own = lax.dynamic_slice_in_dim(values, kv_index * HEAD_DIM, HEAD_DIM, 1)
    out_heads = attn_out.reshape(own_rows, local_heads, HEAD_DIM).astype(jnp.float32)
    grad_heads = grad_out.reshape(own_rows, local_heads, HEAD_DIM).astype(jnp.float32)
    delta_own = jnp.sum(out_heads * grad_heads, axis=2)
    empty_sum = jnp.zeros((src_rows, HEAD_DIM), jnp.float32)
    total_rows = own_rows * lax.axis_size("sp")
    position = lax.axis_index("sp") * own_rows
    delta_full = lax.dynamic_update_slice_in_dim(
        jnp.zeros((total_rows, local_heads), jnp.float32), delta_own, position, 0
    )
    query_all, grad_all = (
        lax.all_gather(queries, "sp", axis=0, tiled=True),
        lax.all_gather(grad_out, "sp", axis=0, tiled=True),
    )
    block_rows = math.gcd(total_rows, 512)
    block_count = total_rows // block_rows
    query_blocks = query_all.reshape(block_count, block_rows, local_heads, HEAD_DIM)
    grad_blocks = grad_all.reshape(block_count, block_rows, local_heads, HEAD_DIM)

    def block_stats(query_block):
        scores = (
            jnp.einsum("qhd,sd->hqs", query_block, key_own, preferred_element_type=jnp.float32)
            * score_scale
        )
        row_peak = jnp.max(scores, axis=2)
        row_total = jnp.sum(jnp.exp(scores - row_peak[:, :, None]), axis=2)
        return (row_peak, row_total)

    peaks, totals = lax.map(block_stats, query_blocks)
    peaks, totals, delta_full = merged((peaks, totals, delta_full), "sp", join_stats)
    log_totals = peaks + jnp.log(totals)
    delta_blocks = delta_full.reshape(block_count, block_rows, local_heads)

    def block_grads(running, inputs):
        query_block, grad_block, delta_block, log_block = inputs
        scores = (
            jnp.einsum("qhd,sd->hqs", query_block, key_own, preferred_element_type=jnp.float32)
            * score_scale
        )
        weights = jnp.exp(scores - log_block[:, :, None])
        grad_weights = jnp.einsum(
            "qhd,sd->hqs", grad_block, value_own, preferred_element_type=jnp.float32
        )
        delta_cols = jnp.transpose(delta_block)
        grad_scores = (weights * (grad_weights - delta_cols[:, :, None]) * score_scale).astype(
            jnp.bfloat16
        )
        key_sum = running[0] + jnp.einsum(
            "hqs,qhd->sd", grad_scores, query_block, preferred_element_type=jnp.float32
        )
        value_sum = running[1] + jnp.einsum(
            "hqs,qhd->sd",
            weights.astype(jnp.bfloat16),
            grad_block,
            preferred_element_type=jnp.float32,
        )
        query_part = jnp.einsum(
            "hqs,sd->qhd", grad_scores, key_own, preferred_element_type=jnp.float32
        )
        return ((key_sum, value_sum), query_part)

    (key_sum, value_sum), query_parts = lax.scan(
        block_grads, (empty_sum, empty_sum), (query_blocks, grad_blocks, delta_blocks, log_totals)
    )
    query_parts = query_parts.reshape(total_rows, 1, local_heads * HEAD_DIM)
    received = lax.all_to_all(
        query_parts.astype(jnp.bfloat16), "sp", split_axis=0, concat_axis=1, tiled=True
    ).astype(query_parts.dtype)
    query_grad = jnp.sum(received, axis=1)
    key_cols = key_sum.reshape(src_rows, 1, HEAD_DIM)
    value_cols = value_sum.reshape(src_rows, 1, HEAD_DIM)
    key_parts, value_parts = (
        lax.all_to_all(
            key_cols.astype(jnp.bfloat16), "tp", split_axis=0, concat_axis=1, tiled=True
        ).astype(key_cols.dtype),
        lax.all_to_all(
            value_cols.astype(jnp.bfloat16), "tp", split_axis=0, concat_axis=1, tiled=True
        ).astype(value_cols.dtype),
    )
    part_rows = key_parts.shape[0]
    per_kv = key_parts.shape[1] // KV_HEADS
    grad_keys = (
        key_parts.reshape(part_rows, KV_HEADS, per_kv, HEAD_DIM)
        .sum(axis=2)
        .reshape(part_rows, KV_HEADS * HEAD_DIM)
    )
    grad_values = (
        value_parts.reshape(part_rows, KV_HEADS, per_kv, HEAD_DIM)
        .sum(axis=2)
        .reshape(part_rows, KV_HEADS * HEAD_DIM)
    )
    query_grad = query_grad.astype(jnp.bfloat16)
    query_all_heads = lax.all_gather(query_grad, "tp", axis=1, tiled=True)
    grad_rows = lax.dot_general(
        query_all_heads, w_query, (((1,), (1,)), ((), ())), preferred_element_type=jnp.float32
    ).astype(jnp.bfloat16)
    target_wide = target.astype(jnp.float32)
    squares = lax.psum(jnp.sum(target_wide * target_wide, axis=1), "tp")
    inverse = lax.rsqrt(squares / WIDTH + norm_eps)
    normed = (target_wide * inverse[:, None] * gain).astype(jnp.bfloat16)
    grad_weight = lax.psum_scatter(
        lax.dot_general(
            normed, query_all_heads, (((0,), (0,)), ((), ())), preferred_element_type=jnp.float32
        ).astype(jnp.bfloat16),
        "sp",
        scatter_dimension=0,
        tiled=True,
    ).astype(jnp.float32)
    return (grad_rows, grad_weight, grad_keys, grad_values)


MESH = pl.DeviceIdType.MESH
BF16, F32 = jnp.bfloat16, jnp.float32
NT = (((1,), (1,)), ((), ()))
X = 2
ZS = 4
CHUNK = 256
NB = 2


def fused_kernel(
    ts, heads,
    target, gain, w_query, queries, keys, values, attn_out, grad_out,
    grad_rows, grad_weight, grad_keys, grad_values,
    qs, dos, outs, kbuf, vbuf, ktr, delta, sbuf, pbuf, dsbuf, qpart, part_in,
    stat, ksum, kv_out, kv_in, kv_tp, kv_tp_in, sq, ntr, nall,
    qown, qmate, qt, dqg, wbuf, res_out, res_in, send, recv, local_sem,
):
    rows = queries.shape[0]
    src = keys.shape[0]
    hd = HEAD_DIM
    width = heads * hd
    half = width // X
    cb = half // NB
    cols = heads * rows
    part = src // ts
    feat = target.shape[1] // (ZS * X)
    scale = hd ** (-0.5)
    sp, tp = lax.axis_index("sp"), lax.axis_index("tp")
    z, x = sp // X, sp % X
    core = tp % 2
    side = z // 2
    outer = 1 - (z + side) % 2
    inner = outer == 0
    z_mate, z_oin, z_oout = 1 + 4 * side - z, 2 - side, 3 - 3 * side
    sib = tp + 1 - 2 * core
    tps = [tp, sib, (tp + 2) % ts, (sib + 2) % ts]
    x_off = 1 - x
    slots_z = [z, z_mate, z_oin, z_oout]

    def dev(zz, xx, tt):
        return (zz * X + xx, tt)

    mate, oin, oout = (dev(a, x, tp) for a in (z_mate, z_oin, z_oout))
    xpeer = dev(z, x_off, tp)
    counts = {"send": 0, "recv": 0, "local": 0}
    pending = []

    def take(kind, n=1):
        at = counts[kind]
        counts[kind] += n
        return at

    def copy_of(source, dest, device, si, ri):
        return pltpu.make_async_remote_copy(
            src_ref=source, dst_ref=dest, send_sem=send.at[si], recv_sem=recv.at[ri],
            device_id=device, device_id_type=MESH,
        )

    def push(source, dest, device, ri, when=None):
        copy = copy_of(source, dest, device, take("send"), ri)
        if when is None:
            copy.start()
        else:
            pl.when(when)(copy.start)
        pending.append((copy, when))

    def arrived(view, ri):
        copy_of(view, view, xpeer, 0, ri).wait_recv()

    def fetch(source, dest):
        copy = pltpu.make_async_copy(source, dest, local_sem.at[take("local")])
        copy.start()
        return copy

    head_col = pl.ds(pl.multiple_of(tp * hd, hd), hd)
    loads = {}
    for name, ref, buf in (("q", queries, qs), ("d", grad_out, dos), ("o", attn_out, outs)):
        loads[name] = []
        for h in range(heads):
            view = buf.at[pl.ds(h * rows, rows)] if buf is outs else buf.at[0, pl.ds(h * rows, rows)]
            loads[name].append(fetch(ref.at[:, pl.ds(h * hd, hd)], view))
    k_load = fetch(keys.at[:, head_col], kbuf.at[pl.ds(0, src)])
    v_load = fetch(values.at[:, head_col], vbuf.at[pl.ds(0, src)])
    w_loads = [
        fetch(w_query.at[:, pl.ds(pl.multiple_of(t * width, width), width)], wbuf.at[e])
        for e, t in enumerate(tps)
    ]

    barrier = pltpu.get_barrier_semaphore()
    peers = [dev(a, x, tp) for a in slots_z[1:]] + [dev(a, x_off, tp) for a in slots_z]
    peers += [dev(z, xx, t) for xx in (x, x_off) for t in tps[1:]]
    for peer in peers:
        pl.semaphore_signal(barrier, inc=1, device_id=peer, device_id_type=MESH)

    wide = target[...].astype(F32)
    sq[0] = jnp.broadcast_to(jnp.sum(wide * wide, axis=1, keepdims=True), (rows, 128))
    for copy in loads["d"] + loads["o"]:
        copy.wait()
    for h in range(heads):
        span = pl.ds(h * rows, rows)
        dot = jnp.sum(dos[0, span].astype(F32) * outs[span].astype(F32), axis=1, keepdims=True)
        delta[0, :, span] = jnp.broadcast_to(dot, (rows, 128)).T[:1]
    for copy in [*loads["q"], k_load, v_load]:
        copy.wait()
    pl.semaphore_wait(barrier, len(peers))

    q_r, d_r, delta_r = take("recv", 4), take("recv", 4), take("recv", 4)
    k_r, v_r = take("recv"), take("recv")
    sq_r = take("recv", 4)

    def gather(buf, base, a, b, device, when=None):
        push(buf.at[a], buf.at[b], device, base + b, when)

    far = 2 + outer
    push(delta.at[0], delta.at[1], mate, delta_r + 1)
    push(delta.at[0], delta.at[far], oin, delta_r + far)
    push(delta.at[0], delta.at[far], oout, delta_r + far)
    for e in range(1, ts):
        push(sq.at[0], sq.at[e], dev(z, x, tps[e]), sq_r + e)
    gather(qs, q_r, 0, 1, mate)
    gather(qs, q_r, 0, 2, oin, inner)
    push(kbuf.at[pl.ds(0, src)], kbuf.at[pl.ds(src, src)], xpeer, k_r)
    gather(dos, d_r, 0, 1, mate)
    gather(dos, d_r, 0, 2, oin, inner)
    push(vbuf.at[pl.ds(0, src)], vbuf.at[pl.ds(src, src)], xpeer, v_r)

    ktr[:, :src] = kbuf[:src].T

    for e in range(1, ts):
        arrived(sq.at[e], sq_r + e)
    total = sq[0]
    for e in range(1, ts):
        total = total + sq[e]
    inverse = lax.rsqrt(total[:, :1] / (target.shape[1] * ts) + norm_eps)
    normed = target[...].astype(F32) * inverse * gain[...]
    ntr[...] = normed.T.astype(BF16)

    def feature_rows(zz, xx):
        return pl.ds(pl.multiple_of((zz * X + xx) * feat, feat), feat)

    def block(xx, t):
        return xx * ts + t

    def lanes(slot, xx):
        return pl.ds(pl.multiple_of((slot * X + xx) * rows, rows), rows)

    n_r = take("recv", ZS * X)
    own = block(x, tp)
    for xr, xx in enumerate((x, x_off)):
        for k, (zz, slot) in enumerate(((z_oin, far), (z_oout, far), (z_mate, 1), (z, 0))):
            if k == 3 and xr == 0:
                continue
            push(
                ntr.at[feature_rows(zz, xx)], nall.at[block(xx, tp), :, lanes(slot, x)],
                dev(zz, xx, tp), n_r + X * slot + xr,
            )
    nall[own, :, lanes(0, x)] = ntr[feature_rows(z, x)]

    def relay(buf, base, a, b, device):
        arrived(buf.at[a], base + a)
        gather(buf, base, a, b, device)

    def relay_inner(buf, base, a, b, device):
        copy = copy_of(buf.at[a], buf.at[b], device, take("send"), base + b)

        @pl.when(inner)
        def _():
            arrived(buf.at[a], base + a)
            copy.start()

        pending.append((copy, inner))

    def arrived_outer(buf, base, a):
        @pl.when(outer > 0)
        def _():
            arrived(buf.at[a], base + a)

    chunks = X * src // CHUNK

    def scores_of(j):
        def step(c, peak):
            span = pl.ds(pl.multiple_of(c * CHUNK, CHUNK), CHUNK)
            s = lax.dot_general(kbuf[span], qs[j], NT, preferred_element_type=F32)
            sbuf[span] = s
            return jnp.maximum(peak, jnp.max(s, axis=0, keepdims=True))

        return lax.fori_loop(0, chunks, step, jnp.full((1, cols), -jnp.inf, F32))

    def grads_of(j, peak):
        own_delta = delta[j]

        def step(c, total):
            span = pl.ds(pl.multiple_of(c * CHUNK, CHUNK), CHUNK)
            p = jnp.exp((sbuf[span] - peak) * scale)
            dp = lax.dot_general(vbuf[span], dos[j], NT, preferred_element_type=F32)
            pbuf[j, span] = p.astype(BF16)
            dsbuf[j, span] = (p * (dp - own_delta) * scale).astype(BF16)
            return total + jnp.sum(p, axis=0, keepdims=True)

        total = lax.fori_loop(0, chunks, step, jnp.zeros((1, cols), F32))
        stat[0, slots_z[j], 0:1] = peak * scale
        stat[0, slots_z[j], 1:2] = total
        qpart[j] = jnp.dot(ktr[...], dsbuf[j], preferred_element_type=F32).astype(BF16)

    stat_r, part_r = take("recv", ZS * ZS), take("recv", 6)

    def share(j):
        zt = slots_z[j]
        push(stat.at[0, zt], stat.at[far, zt], oin, stat_r + ZS * far + j)
        push(stat.at[0, zt], stat.at[1, zt], mate, stat_r + ZS + j)
        push(stat.at[0, zt], stat.at[far, zt], oout, stat_r + ZS * far + j)
        if j < 2:
            push(qpart.at[j], part_in.at[0, 1 - j], mate, part_r + 1 - j, outer > 0)
        else:
            i = far - 1
            push(qpart.at[j], part_in.at[i, j - 2], oin, part_r + 2 * i + j - 2)

    arrived(kbuf.at[pl.ds(src, src)], k_r)
    ktr[:, src:] = kbuf[src:].T
    arrived_outer(qs, q_r, 1)
    relay_inner(qs, q_r, 1, 3, oin)
    relay_inner(qs, q_r, 2, 2, mate)
    peak = scores_of(0)
    arrived_outer(dos, d_r, 1)
    relay_inner(dos, d_r, 1, 3, oin)
    relay_inner(dos, d_r, 2, 2, mate)
    arrived(vbuf.at[pl.ds(src, src)], v_r)
    grads_of(0, peak)
    share(0)
    arrived(delta.at[1], delta_r + 1)
    grads_of(1, scores_of(1))
    share(1)
    relay_inner(qs, q_r, 3, 3, mate)
    arrived_outer(qs, q_r, 2)
    for j in (2, 3):
        arrived(delta.at[j], delta_r + j)
    peak = scores_of(2)
    arrived_outer(dos, d_r, 2)
    grads_of(2, peak)
    share(2)
    relay_inner(dos, d_r, 3, 3, mate)
    for slot in range(ZS):
        for xr in range(X):
            if slot or xr:
                arrived(nall.at[0, :, pl.ds(0, rows)], n_r + X * slot + xr)
    n2_r, n3_r = take("recv", 4), take("recv", 4)
    places = [(x, tps[0]), (x_off, tps[0]), (x, tps[2]), (x_off, tps[2])]
    for i in (3, 1, 2):
        push(nall.at[own], nall.at[own], dev(z, *places[i]), n2_r + i)
    push(nall.at[own], nall.at[own], dev(z, x, sib), n3_r)
    arrived_outer(qs, q_r, 3)
    peak = scores_of(3)
    arrived_outer(dos, d_r, 3)
    grads_of(3, peak)
    share(3)

    def factors(j):
        zt = slots_z[j]
        tops = [stat[e, zt, 0:1] for e in range(ZS)]
        top = functools.reduce(jnp.maximum, tops)
        scaled = [jnp.exp(m - top) for m in tops]
        summed = sum(f * stat[e, zt, 1:2] for e, f in enumerate(scaled))
        return [f / summed for f in scaled]

    def reduced(j, out):
        f = factors(j)
        grad_t = qpart[j].astype(F32) * f[0]
        for i in range(3):
            arrived(part_in.at[i, j], part_r + 2 * i + j)
            grad_t = grad_t + part_in[i, j].astype(F32) * f[i + 1]
        grad_own = grad_t.T
        for h in range(heads):
            out[:, pl.ds(h * hd, hd)] = grad_own[h * rows : (h + 1) * rows].astype(BF16)

    xs_r = take("recv", 2 * NB)
    g_r = take("recv", ZS * NB)
    qt_r = take("recv", ts)
    own_r = take("recv")

    def rows_of(slot, xx):
        return pl.ds(pl.multiple_of((slot * X + xx) * rows, rows), rows)

    def g_view(b, slot):
        return dqg.at[b, pl.ds(slot * X * rows, X * rows)]

    def col_of(xx, b):
        return pl.ds(pl.multiple_of(xx * half + b * cb, cb), cb)

    def spread(slot, buf, when=None):
        for b in range(NB):
            push(
                buf.at[:, col_of(x_off, b)], dqg.at[b, rows_of(slot, x)], xpeer,
                xs_r + slot * NB + b, when,
            )

    def keep(slot, buf):
        for b in range(NB):
            dqg[b, rows_of(slot, x)] = buf[:, col_of(x, b)]

    def joined(slot, b):
        arrived(dqg.at[b, pl.ds(0, rows)], xs_r + slot * NB + b)

    def hand(slot, to, b, device):
        push(g_view(b, slot), g_view(b, to), device, g_r + ZS * b + to, inner)

    def came(slot, b):
        arrived(g_view(b, slot), g_r + ZS * b + slot)

    def qt_sends(when):
        push(qown, qt.at[2], dev(z, x, tps[2]), qt_r + 2, when)
        push(qown, qt.at[1], dev(z, x, sib), qt_r + 1, when)

    arrived(stat.at[1, 0], stat_r + ZS + 1)
    arrived(stat.at[2, 0], stat_r + ZS * 2 + 2)
    arrived(stat.at[3, 0], stat_r + ZS * 3 + 2)

    @pl.when(inner)
    def _():
        reduced(0, qown)
        keep(0, qown)

    spread(0, qown, inner)
    qt_sends(inner)
    for i in (1, 2, 3):
        xx, t = places[i]
        arrived(nall.at[0], n2_r + i)
        push(nall.at[block(xx, t)], nall.at[block(xx, t)], dev(z, x, sib), n3_r + i)
    for b in range(NB):
        @pl.when(inner)
        def _():
            joined(0, b)

        hand(0, 2, b, oin)
        hand(0, 1, b, mate)

    for e, js in ((1, (0, 2, 3)), (2, (0, 1, 3)), (3, (0, 1, 3))):
        for j in js:
            arrived(stat.at[e, 0], stat_r + ZS * e + j)

    @pl.when(inner)
    def _():
        reduced(1, qmate)

    push(qmate, qown, mate, own_r, inner)
    spread(1, qmate, inner)

    @pl.when(inner)
    def _():
        keep(1, qmate)

    for j in range(ZS):
        r = factors(j)[0]
        r = jnp.broadcast_to(r, (128, cols)).T
        r = jnp.concatenate([r] * (hd // 128), axis=1)
        q_scaled = (qs[j].astype(F32) * r).astype(BF16)
        d_scaled = (dos[j].astype(F32) * r).astype(BF16)
        for i, (left, right) in enumerate(((dsbuf, q_scaled), (pbuf, d_scaled))):
            piece = jnp.dot(left[j], right, preferred_element_type=F32)
            ksum[i] = piece if j == 0 else ksum[i] + piece
    kv_out[...] = ksum[:, src:].astype(BF16)
    kvx_r = take("recv")
    push(kv_out, kv_in, xpeer, kvx_r)

    def pass_on(slot, b):
        copy = copy_of(g_view(b, slot), g_view(b, slot), mate, take("send"), g_r + ZS * b + slot)

        @pl.when(inner)
        def _():
            came(slot, b)
            copy.start()

        pending.append((copy, inner))

    for b in range(NB):
        pass_on(2, b)

        @pl.when(inner)
        def _():
            joined(1, b)

        hand(1, 3, b, oin)
    @pl.when(outer > 0)
    def _():
        arrived(qown, own_r)
        keep(0, qown)

    spread(0, qown, outer > 0)
    qt_sends(outer > 0)

    arrived(kv_in, kvx_r)
    for i in range(2):
        ksum[i, :src] = ksum[i, :src] + kv_in[i].astype(F32)
    kv_tp[...] = ksum[:, :src].astype(BF16)

    def part_rows(t):
        return pl.ds(pl.multiple_of(t * part, part), part)

    kvt_r = take("recv", ts)
    for e in range(1, ts):
        push(kv_tp.at[:, part_rows(tps[e])], kv_tp_in.at[e], dev(z, x, tps[e]), kvt_r + e)
    for i, out in enumerate((grad_keys, grad_values)):
        out[:, head_col] = ksum[i, part_rows(tp)]

    w_loads[0].wait()
    rows_sum = lax.dot_general(qown[...], wbuf[0], NT, preferred_element_type=F32)
    arrived(qt.at[2], qt_r + 2)
    push(qt.at[2], qt.at[3], dev(z, x, sib), qt_r + 3)
    for i in range(4):
        arrived(nall.at[0], n3_r + i)

    res_r = take("recv", NB * X * ts)
    order = [(1, 3), (1, 2), (0, 3), (0, 2), (1, 1), (1, 0), (0, 1), (0, 0)]

    def project(b):
        for xr, e in order:
            xx, k = (x, x_off)[xr], xr * ts + e
            piece = jnp.dot(nall[block(xx, tps[e])], dqg[b], preferred_element_type=F32)
            if k:
                res_out[b, k] = piece.astype(BF16)
                push(
                    res_out.at[b, k], res_in.at[b, k], dev(z, xx, tps[e]),
                    res_r + b * X * ts + k,
                )
            else:
                at = pl.multiple_of(tp * width + x * half + b * cb, cb)
                grad_weight[:, pl.ds(at, cb)] = piece

    for b in range(NB):
        @pl.when(outer > 0)
        def _():
            joined(0, b)
            came(1, b)
            came(2, b)
            came(3, b)

        pass_on(3, b)
        project(b)

    for e in (1, 2, 3):
        if e != 2:
            arrived(qt.at[e], qt_r + e)
        w_loads[e].wait()
        rows_sum = rows_sum + lax.dot_general(qt[e], wbuf[e], NT, preferred_element_type=F32)
    grad_rows[...] = rows_sum.astype(BF16)
    for e in range(1, ts):
        arrived(kv_tp_in.at[e], kvt_r + e)
        at = pl.ds(pl.multiple_of(tps[e] * hd, hd), hd)
        for i, out in enumerate((grad_keys, grad_values)):
            out[:, at] = kv_tp_in[e, i].astype(F32)
    for b in range(NB):
        for xr, e in order[:-1]:
            xx, k = (x, x_off)[xr], xr * ts + e
            arrived(res_in.at[b, k], res_r + b * X * ts + k)
            at = pl.multiple_of(tps[e] * width + xx * half + b * cb, cb)
            grad_weight[:, pl.ds(at, cb)] = res_in[b, k].astype(F32)
    for copy, when in pending:
        if when is None:
            copy.wait_send()
        else:
            pl.when(when)(copy.wait_send)


def fused(target, gain, w_query, queries, keys, values, attn_out, grad_out):
    ts = lax.axis_size("tp")
    rows, width = queries.shape
    src = keys.shape[0]
    heads = width // HEAD_DIM
    cols, hd = heads * rows, HEAD_DIM
    feats = target.shape[1]
    feat = feats // (ZS * X)
    part = src // ts
    cb = width // X // NB
    vmem, hbm = pl.BlockSpec(memory_space=pltpu.VMEM), pl.BlockSpec(memory_space=pl.ANY)
    return pl.pallas_call(
        functools.partial(fused_kernel, ts, heads),
        out_shape=(
            jax.ShapeDtypeStruct((rows, feats), BF16),
            jax.ShapeDtypeStruct((feat, width * ts), F32),
            jax.ShapeDtypeStruct((part, keys.shape[1]), F32),
            jax.ShapeDtypeStruct((part, keys.shape[1]), F32),
        ),
        in_specs=[vmem, vmem, hbm, hbm, hbm, hbm, hbm, hbm],
        out_specs=(vmem,) * 4,
        scratch_shapes=[
            pltpu.VMEM((ZS, cols, hd), BF16),
            pltpu.VMEM((ZS, cols, hd), BF16),
            pltpu.VMEM((cols, hd), BF16),
            pltpu.VMEM((X * src, hd), BF16),
            pltpu.VMEM((X * src, hd), BF16),
            pltpu.VMEM((hd, X * src), BF16),
            pltpu.VMEM((ZS, 1, cols), F32),
            pltpu.VMEM((X * src, cols), F32),
            pltpu.VMEM((ZS, X * src, cols), BF16),
            pltpu.VMEM((ZS, X * src, cols), BF16),
            pltpu.VMEM((ZS, hd, cols), BF16),
            pltpu.VMEM((3, 2, hd, cols), BF16),
            pltpu.VMEM((ZS, ZS, 2, cols), F32),
            pltpu.VMEM((2, X * src, hd), F32),
            pltpu.VMEM((2, src, hd), BF16),
            pltpu.VMEM((2, src, hd), BF16),
            pltpu.VMEM((2, src, hd), BF16),
            pltpu.VMEM((ts, 2, part, hd), BF16),
            pltpu.VMEM((ts, rows, 128), F32),
            pltpu.VMEM((feats, rows), BF16),
            pltpu.VMEM((X * ts, feat, ZS * X * rows), BF16),
            pltpu.VMEM((rows, width), BF16),
            pltpu.VMEM((rows, width), BF16),
            pltpu.VMEM((ts, rows, width), BF16),
            pltpu.VMEM((NB, ZS * X * rows, cb), BF16),
            pltpu.VMEM((ts, feats, width), BF16),
            pltpu.VMEM((NB, X * ts, feat, cb), BF16),
            pltpu.VMEM((NB, X * ts, feat, cb), BF16),
            pltpu.SemaphoreType.DMA((96 + 24 * NB,)),
            pltpu.SemaphoreType.DMA((80 + 14 * NB,)),
            pltpu.SemaphoreType.DMA((2 + 3 * heads + ts,)),
        ],
        compiler_params=pltpu.CompilerParams(
            collective_id=0, has_side_effects=True, vmem_limit_bytes=60 * 2**20
        ),
    )(target, gain.reshape(1, feats), w_query, queries, keys, values, attn_out, grad_out)


def fits(mesh):
    sp, tp = mesh.shape["sp"], mesh.shape["tp"]
    feat = WIDTH // (sp * tp)
    return tp == KV_HEADS and sp == ZS * X and feat % 128 == 0


def solution(mesh):
    return jax.shard_map(
        fused if fits(mesh) else local,
        mesh=mesh,
        in_specs=(
            P("sp", "tp"),
            P("tp"),
            P("tp", None),
            P("sp", "tp"),
            P("sp", None),
            P("sp", None),
            P("sp", "tp"),
            P("sp", "tp"),
        ),
        out_specs=(
            P("sp", "tp"),
            P(("tp", "sp"), None),
            P(("sp", "tp"), None),
            P(("sp", "tp"), None),
        ),
        check_vma=False,
    )
```

time: 136 us -> 105 us (0.77)
  Pallas kernels: 126 us -> 96.4 us
    pallas_call x1, Pallas kernels: 126 us -> 96.4 us  [fused(): pl.pallas_call(functools.partial(fused_kernel, ts, heads), out_shape=(jax...]
where the time goes in v1:
time: 105 us; the launch traced here: 104 us
  Pallas kernels  96.4 us (92%)
  local copies, waits for them, and re-layouts  6.46 us (6%)
    pallas_call x1, Pallas kernels, fused(): pl.pallas_call(functools.partial(fused_kernel, ts, heads), out_shape=(jax...  96.4 us
    unnamed x8, local copies, waits for them, and re-layouts  6.46 us

profile of v1, /device:TPU:1, one launch (start us, length us, event | category | flops | bytes accessed | tf_op | source)
XLA Modules:
  0.0 103.5 jit_solution(2261711959336836267)
XLA Ops:
  0.6 96.4 %shard_map.111 = (bf16[128,1024]{1,0:T(8,128)(2,1)}, f32[128,4096]{1,0:T(8,128)}, f32[128,1024]{1,0:T(8,128)}, f32[128,1024]{1,0:T(8,128)}) custom-call(bf16[128,1024]{1,0:T(8,128)(2,1)} %target.1, f32[1,1024]{1,0:T(1,128)} %bitcast.1, bf16[1024,4096]{1,0:T(8,128)(2,1)} %w_query.1, bf16[128,1024]{1,0:T(8,128)(2,1)} %queries.1, bf16[512,1024]{1,0:T(8,128)(2,1)} %keys.1, ...), custom_call_target="tpu_custom_call" | custom-call | tf_op jit(solution)/shard_map/pallas_call | solution.py:631
  97.0 1.7 %copy.16 = bf16[128,1024]{1,0:T(8,128)(2,1)} copy(bf16[128,1024]{1,0:T(8,128)(2,1)} %get-tuple-element.8) | data formatting | bytes 524288
  98.7 0.0 copy-start.1
  98.7 0.0 copy-start
  98.7 3.2 %copy.17 = f32[128,4096]{1,0:T(8,128)} copy(f32[128,4096]{1,0:T(8,128)} %get-tuple-element.9) | data formatting | bytes 4194304
  101.9 0.0 copy-done.1
  101.9 0.8 copy.18
  102.7 0.0 copy-done
  102.7 0.8 copy.19
Async XLA Ops:
  98.7 3.2 %copy-start.1 = (f32[128,1024]{1,0:T(8,128)S(1)}, f32[128,1024]{1,0:T(8,128)}, u32[]{:S(2)}) copy-start(f32[128,1024]{1,0:T(8,128)} %get-tuple-element.10) | copy-start | bytes 1572868
  98.7 4.0 %copy-start = (f32[128,1024]{1,0:T(8,128)S(1)}, f32[128,1024]{1,0:T(8,128)}, u32[]{:S(2)}) copy-start(f32[128,1024]{1,0:T(8,128)} %get-tuple-element.11) | copy-start | bytes 1572868

commit v2 on v1

v2 whole, which is shorter than its diff:
```python
import functools
import math

import jax
import jax.numpy as jnp
from jax import lax
from jax.experimental import pallas as pl
from jax.experimental.pallas import tpu as pltpu
from jax.sharding import PartitionSpec as P

WIDTH = 4096
HEADS = 16
KV_HEADS = 4
HEAD_DIM = 256


norm_eps = 1e-06


def merged(part, axis, combine):
    gathered = jax.tree.map(lambda a: lax.all_gather(a, axis), part)

    def take(source):
        return jax.tree.map(lambda a: lax.dynamic_index_in_dim(a, source, 0, False), gathered)

    return lax.fori_loop(
        1, lax.axis_size(axis), lambda source, state: combine(state, take(source)), take(0)
    )


def join_stats(first_part, second_part):
    row_peak = jnp.maximum(first_part[0], second_part[0])
    summed = first_part[1] * jnp.exp(first_part[0] - row_peak) + second_part[1] * jnp.exp(
        second_part[0] - row_peak
    )
    return (row_peak, summed, first_part[2] + second_part[2])


def local(target, gain, w_query, queries, keys, values, attn_out, grad_out):
    local_heads = queries.shape[1] // HEAD_DIM
    group_size = HEADS // KV_HEADS
    score_scale = HEAD_DIM ** (-0.5)
    own_rows = queries.shape[0]
    src_rows = keys.shape[0]
    kv_index = lax.axis_index("tp") * local_heads // group_size
    key_own = lax.dynamic_slice_in_dim(keys, kv_index * HEAD_DIM, HEAD_DIM, 1)
    value_own = lax.dynamic_slice_in_dim(values, kv_index * HEAD_DIM, HEAD_DIM, 1)
    out_heads = attn_out.reshape(own_rows, local_heads, HEAD_DIM).astype(jnp.float32)
    grad_heads = grad_out.reshape(own_rows, local_heads, HEAD_DIM).astype(jnp.float32)
    delta_own = jnp.sum(out_heads * grad_heads, axis=2)
    empty_sum = jnp.zeros((src_rows, HEAD_DIM), jnp.float32)
    total_rows = own_rows * lax.axis_size("sp")
    position = lax.axis_index("sp") * own_rows
    delta_full = lax.dynamic_update_slice_in_dim(
        jnp.zeros((total_rows, local_heads), jnp.float32), delta_own, position, 0
    )
    query_all, grad_all = (
        lax.all_gather(queries, "sp", axis=0, tiled=True),
        lax.all_gather(grad_out, "sp", axis=0, tiled=True),
    )
    block_rows = math.gcd(total_rows, 512)
    block_count = total_rows // block_rows
    query_blocks = query_all.reshape(block_count, block_rows, local_heads, HEAD_DIM)
    grad_blocks = grad_all.reshape(block_count, block_rows, local_heads, HEAD_DIM)

    def block_stats(query_block):
        scores = (
            jnp.einsum("qhd,sd->hqs", query_block, key_own, preferred_element_type=jnp.float32)
            * score_scale
        )
        row_peak = jnp.max(scores, axis=2)
        row_total = jnp.sum(jnp.exp(scores - row_peak[:, :, None]), axis=2)
        return (row_peak, row_total)

    peaks, totals = lax.map(block_stats, query_blocks)
    peaks, totals, delta_full = merged((peaks, totals, delta_full), "sp", join_stats)
    log_totals = peaks + jnp.log(totals)
    delta_blocks = delta_full.reshape(block_count, block_rows, local_heads)

    def block_grads(running, inputs):
        query_block, grad_block, delta_block, log_block = inputs
        scores = (
            jnp.einsum("qhd,sd->hqs", query_block, key_own, preferred_element_type=jnp.float32)
            * score_scale
        )
        weights = jnp.exp(scores - log_block[:, :, None])
        grad_weights = jnp.einsum(
            "qhd,sd->hqs", grad_block, value_own, preferred_element_type=jnp.float32
        )
        delta_cols = jnp.transpose(delta_block)
        grad_scores = (weights * (grad_weights - delta_cols[:, :, None]) * score_scale).astype(
            jnp.bfloat16
        )
        key_sum = running[0] + jnp.einsum(
            "hqs,qhd->sd", grad_scores, query_block, preferred_element_type=jnp.float32
        )
        value_sum = running[1] + jnp.einsum(
            "hqs,qhd->sd",
            weights.astype(jnp.bfloat16),
            grad_block,
            preferred_element_type=jnp.float32,
        )
        query_part = jnp.einsum(
            "hqs,sd->qhd", grad_scores, key_own, preferred_element_type=jnp.float32
        )
        return ((key_sum, value_sum), query_part)

    (key_sum, value_sum), query_parts = lax.scan(
        block_grads, (empty_sum, empty_sum), (query_blocks, grad_blocks, delta_blocks, log_totals)
    )
    query_parts = query_parts.reshape(total_rows, 1, local_heads * HEAD_DIM)
    received = lax.all_to_all(
        query_parts.astype(jnp.bfloat16), "sp", split_axis=0, concat_axis=1, tiled=True
    ).astype(query_parts.dtype)
    query_grad = jnp.sum(received, axis=1)
    key_cols = key_sum.reshape(src_rows, 1, HEAD_DIM)
    value_cols = value_sum.reshape(src_rows, 1, HEAD_DIM)
    key_parts, value_parts = (
        lax.all_to_all(
            key_cols.astype(jnp.bfloat16), "tp", split_axis=0, concat_axis=1, tiled=True
        ).astype(key_cols.dtype),
        lax.all_to_all(
            value_cols.astype(jnp.bfloat16), "tp", split_axis=0, concat_axis=1, tiled=True
        ).astype(value_cols.dtype),
    )
    part_rows = key_parts.shape[0]
    per_kv = key_parts.shape[1] // KV_HEADS
    grad_keys = (
        key_parts.reshape(part_rows, KV_HEADS, per_kv, HEAD_DIM)
        .sum(axis=2)
        .reshape(part_rows, KV_HEADS * HEAD_DIM)
    )
    grad_values = (
        value_parts.reshape(part_rows, KV_HEADS, per_kv, HEAD_DIM)
        .sum(axis=2)
        .reshape(part_rows, KV_HEADS * HEAD_DIM)
    )
    query_grad = query_grad.astype(jnp.bfloat16)
    query_all_heads = lax.all_gather(query_grad, "tp", axis=1, tiled=True)
    grad_rows = lax.dot_general(
        query_all_heads, w_query, (((1,), (1,)), ((), ())), preferred_element_type=jnp.float32
    ).astype(jnp.bfloat16)
    target_wide = target.astype(jnp.float32)
    squares = lax.psum(jnp.sum(target_wide * target_wide, axis=1), "tp")
    inverse = lax.rsqrt(squares / WIDTH + norm_eps)
    normed = (target_wide * inverse[:, None] * gain).astype(jnp.bfloat16)
    grad_weight = lax.psum_scatter(
        lax.dot_general(
            normed, query_all_heads, (((0,), (0,)), ((), ())), preferred_element_type=jnp.float32
        ).astype(jnp.bfloat16),
        "sp",
        scatter_dimension=0,
        tiled=True,
    ).astype(jnp.float32)
    return (grad_rows, grad_weight, grad_keys, grad_values)


MESH = pl.DeviceIdType.MESH
BF16, F32 = jnp.bfloat16, jnp.float32
NT = (((1,), (1,)), ((), ()))
X = 2
ZS = 4
CHUNK = 512
PIECES = 4


def fused_kernel(
    ts, heads,
    target, gain, w_query, queries, keys, values, attn_out, grad_out,
    rows_raw, weight_raw, kv_raw,
    qs, dos, outs, kbuf, vbuf, ktr, delta, sbuf, pbuf, dsbuf, qpart, part_in,
    side_out, side_in, stat, ksum, kv_out, kv_in, kv_tp, sq, ntr, nall,
    dqrow, qt, dqg, wbuf, res_out, rows_out, send, recv, local_sem,
):
    rows = queries.shape[0]
    src = keys.shape[0]
    hd = HEAD_DIM
    width = heads * hd
    groups = heads // X
    half = width // X
    gcols = X * rows
    part = src // ts
    feat = target.shape[1] // (ZS * X)
    scale = hd ** (-0.5)
    sp, tp = lax.axis_index("sp"), lax.axis_index("tp")
    z, x = sp // X, sp % X
    core = tp % 2
    side = z // 2
    outer = 1 - (z + side) % 2
    inner = outer == 0
    edge = outer > 0
    z_mate, z_oin, z_oout = 1 + 4 * side - z, 2 - side, 3 - 3 * side
    sib = tp + 1 - 2 * core
    tps = [tp, sib, (tp + 2) % ts, (sib + 2) % ts]
    x_off = 1 - x
    slots_z = [z, z_mate, z_oin, z_oout]
    swap = (1, 0, 2, 3)
    far = 2 + outer

    def dev(zz, xx, tt):
        return (zz * X + xx, tt)

    mate, oin, oout = (dev(a, x, tp) for a in (z_mate, z_oin, z_oout))
    xpeer, y_peer, sib_peer = dev(z, x_off, tp), dev(z, x, tps[2]), dev(z, x, sib)
    counts = {"send": 0, "recv": 0, "local": 0}
    pending = []

    def take(kind, n=1):
        at = counts[kind]
        counts[kind] += n
        return at

    def copy_of(source, dest, device, si, ri):
        return pltpu.make_async_remote_copy(
            src_ref=source, dst_ref=dest, send_sem=send.at[si], recv_sem=recv.at[ri],
            device_id=device, device_id_type=MESH,
        )

    def push(source, dest, device, ri, when=None):
        copy = copy_of(source, dest, device, take("send"), ri)
        if when is None:
            copy.start()
        else:
            pl.when(when)(copy.start)
        pending.append((copy, when))

    def arrived(view, ri):
        copy_of(view, view, xpeer, 0, ri).wait_recv()

    def fetch(source, dest):
        copy = pltpu.make_async_copy(source, dest, local_sem.at[take("local")])
        copy.start()
        return copy

    def head_of(g, xx):
        return xx * groups + g

    head_col = pl.ds(pl.multiple_of(tp * hd, hd), hd)
    loads = {"q": [], "d": [], "o": []}
    for name, ref, buf in (("q", queries, qs), ("d", grad_out, dos), ("o", attn_out, outs)):
        for g in range(groups):
            for xx in range(X):
                view = buf.at[g] if buf is outs else buf.at[g, 0]
                view = view.at[pl.ds(xx * rows, rows)]
                loads[name].append(fetch(ref.at[:, pl.ds(head_of(g, xx) * hd, hd)], view))
    k_load = fetch(keys.at[:, head_col], kbuf.at[pl.ds(0, src)])
    v_load = fetch(values.at[:, head_col], vbuf.at[pl.ds(0, src)])
    w_loads = [
        fetch(w_query.at[:, pl.ds(pl.multiple_of(t * width, width), width)], wbuf.at[e])
        for e, t in enumerate(tps)
    ]

    barrier = pltpu.get_barrier_semaphore()
    peers = [dev(a, x, tp) for a in slots_z[1:]] + [dev(a, x_off, tp) for a in slots_z]
    peers += [dev(z, xx, t) for xx in (x, x_off) for t in tps[1:]]
    for peer in peers:
        pl.semaphore_signal(barrier, inc=1, device_id=peer, device_id_type=MESH)

    wide = target[...].astype(F32)
    sq[0] = jnp.broadcast_to(jnp.sum(wide * wide, axis=1, keepdims=True), (rows, 128))
    for copy in loads["d"] + loads["o"]:
        copy.wait()
    for g in range(groups):
        dot = jnp.sum(dos[g, 0].astype(F32) * outs[g].astype(F32), axis=1, keepdims=True)
        delta[0, g] = jnp.broadcast_to(dot, (gcols, 128)).T[:1]
    for copy in [*loads["q"], k_load, v_load]:
        copy.wait()
    pl.semaphore_wait(barrier, len(peers))

    q_r, d_r = take("recv", ZS * groups), take("recv", ZS * groups)
    delta_r, sq_r = take("recv", ZS), take("recv", ZS)
    k_r, v_r = take("recv"), take("recv")

    def gather(buf, base, g, a, b, device, when=None):
        push(buf.at[g, a], buf.at[g, b], device, base + ZS * g + b, when)

    push(delta.at[0], delta.at[1], mate, delta_r + 1)
    push(delta.at[0], delta.at[far], oin, delta_r + far)
    push(delta.at[0], delta.at[far], oout, delta_r + far)
    for e in range(1, ts):
        push(sq.at[0], sq.at[e], dev(z, x, tps[e]), sq_r + e)
    gather(qs, q_r, 0, 0, 1, mate)
    gather(qs, q_r, 0, 0, 2, oin, inner)
    push(kbuf.at[pl.ds(0, src)], kbuf.at[pl.ds(src, src)], xpeer, k_r)
    gather(dos, d_r, 0, 0, 1, mate)
    gather(dos, d_r, 0, 0, 2, oin, inner)
    push(vbuf.at[pl.ds(0, src)], vbuf.at[pl.ds(src, src)], xpeer, v_r)
    for g in range(1, groups):
        gather(qs, q_r, g, 0, 1, mate)
        gather(dos, d_r, g, 0, 1, mate)

    ktr[:, :src] = kbuf[:src].T
    for e in range(1, ts):
        arrived(sq.at[e], sq_r + e)
    total = sq[0]
    for e in range(1, ts):
        total = total + sq[e]
    inverse = lax.rsqrt(total[:, :1] / (target.shape[1] * ts) + norm_eps)
    normed = target[...].astype(F32) * inverse * gain[...]
    ntr[...] = normed.T.astype(BF16)

    def feature_rows(zz, xx):
        return pl.ds(pl.multiple_of((zz * X + xx) * feat, feat), feat)

    def lanes(slot, xx):
        return pl.ds(pl.multiple_of((slot * X + xx) * rows, rows), rows)

    n_r = take("recv", ZS * X)
    n_in = take("recv", X * ts)

    def n_send(zz, slot, xr):
        xx = (x, x_off)[xr]
        push(
            ntr.at[feature_rows(zz, xx)], nall.at[0, :, lanes(slot, x)], dev(zz, xx, tp),
            n_r + X * slot + xr,
        )

    def n_pass(i, to, device, when=None):
        push(nall.at[i], nall.at[to], device, n_in + to, when)

    def n_relay(when):
        @pl.when(when)
        def _():
            arrived(nall.at[0], n_in + ts)

        n_pass(ts, ts + 2, y_peer, when)
        n_pass(ts, ts + 1, sib_peer, when)

    nall[0, :, lanes(0, x)] = ntr[feature_rows(z, x)]

    def relay(g, a, b, device):
        for buf, base in ((qs, q_r), (dos, d_r)):
            copy = copy_of(
                buf.at[g, a], buf.at[g, b], device, take("send"), base + ZS * g + b
            )

            @pl.when(inner)
            def _():
                arrived(buf.at[g, a], base + ZS * g + a)
                copy.start()

            pending.append((copy, inner))

    def gathered(g, a):
        @pl.when(edge)
        def _():
            arrived(qs.at[g, a], q_r + ZS * g + a)
            arrived(dos.at[g, a], d_r + ZS * g + a)

    chunks = X * src // CHUNK

    def scores_of(g, j):
        def step(c, peak):
            span = pl.ds(pl.multiple_of(c * CHUNK, CHUNK), CHUNK)
            s = lax.dot_general(kbuf[span], qs[g, j], NT, preferred_element_type=F32)
            sbuf[span] = s
            return jnp.maximum(peak, jnp.max(s, axis=0, keepdims=True))

        return lax.fori_loop(0, chunks, step, jnp.full((1, gcols), -jnp.inf, F32), unroll=True)

    def grads_of(g, j, peak):
        own_delta = delta[j, g]
        lane_span = pl.ds((g * ZS + j) * gcols, gcols)

        def step(c, total):
            span = pl.ds(pl.multiple_of(c * CHUNK, CHUNK), CHUNK)
            p = jnp.exp((sbuf[span] - peak) * scale)
            dp = lax.dot_general(vbuf[span], dos[g, j], NT, preferred_element_type=F32)
            pbuf[span, lane_span] = p.astype(BF16)
            dsbuf[span, lane_span] = (p * (dp - own_delta) * scale).astype(BF16)
            return total + jnp.sum(p, axis=0, keepdims=True)

        total = lax.fori_loop(0, chunks, step, jnp.zeros((1, gcols), F32), unroll=True)
        stat[0, slots_z[j], g, 0:1] = peak * scale
        stat[0, slots_z[j], g, 1:2] = total
        qpart[g, j] = jnp.dot(ktr[...], dsbuf[:, lane_span], preferred_element_type=F32).astype(BF16)

    stat_r = take("recv", groups * ZS * ZS)
    part_r, side_r = take("recv", groups * ZS), take("recv", groups * ZS)

    def stat_at(g, e, j):
        return stat_r + ZS * ZS * g + ZS * e + j

    def share(g, j):
        zt = slots_z[j]
        for e, device in ((far, oin), (far, oout), (1, mate)):
            push(stat.at[0, zt, g], stat.at[e, zt, g], device, stat_at(g, e, j))
        to = swap[j]
        push(qpart.at[g, j], part_in.at[g, to], mate, part_r + ZS * g + to, edge)

    def process(g, j):
        grads_of(g, j, scores_of(g, j))
        share(g, j)

    def weights_of(g, j, sources):
        zt = slots_z[j]
        tops = [stat[e, zt, g, 0:1] for e in sources]
        top = functools.reduce(jnp.maximum, tops)
        scaled = [jnp.exp(m - top) for m in tops]
        summed = sum(f * stat[e, zt, g, 1:2] for e, f in zip(sources, scaled))
        return top, scaled, summed

    def stats_came(g, j):
        there = (j + 2) % ZS
        for e, k in ((2, there), (3, there if there > 1 else swap[there])):
            arrived(stat.at[0, 0, 0], stat_at(g, e, k))

    def side_sum(g, j):
        @pl.when(inner)
        def _():
            arrived(stat.at[0, 0, 0], stat_at(g, 1, swap[j]))
            arrived(part_in.at[g, j], part_r + ZS * g + j)
            _, (f_own, f_mate), _ = weights_of(g, j, (0, 1))
            near_part = qpart[g, j].astype(F32) * f_own + part_in[g, j].astype(F32) * f_mate
            side_out[g, j] = near_part.astype(BF16)

        to = (j + 2) % ZS
        push(side_out.at[g, j], side_in.at[g, to], oin, side_r + ZS * g + to, inner)

    row_r, xs_r, g_r = (take("recv", groups * ZS) for _ in range(3))
    qt_r = take("recv", ts * groups)

    def rows_of(slot, xx):
        return pl.ds(pl.multiple_of((slot * X + xx) * rows, rows), rows)

    def lanes_of(xx):
        return pl.ds(pl.multiple_of(xx * hd, hd), hd)

    def spread(g, j, when):
        push(
            dqrow.at[g, j, :, lanes_of(x_off)], dqg.at[g, rows_of(j, x)], xpeer,
            xs_r + ZS * g + j, when,
        )

        @pl.when(when)
        def _():
            dqg[g, rows_of(j, x)] = dqrow[g, j, :, lanes_of(x)]

    def qt_sends(g, when):
        push(dqrow.at[g, 0], qt.at[2, g], y_peer, qt_r + groups * 2 + g, when)
        push(dqrow.at[g, 0], qt.at[1, g], sib_peer, qt_r + groups + g, when)

    def reduce_rows(g, j):
        @pl.when(inner)
        def _():
            arrived(side_in.at[g, j], side_r + ZS * g + j)
            top, _, summed = weights_of(g, j, range(ZS))
            near_top, far_top = (weights_of(g, j, pair)[0] for pair in ((0, 1), (2, 3)))
            grad_t = side_out[g, j].astype(F32) * (jnp.exp(near_top - top) / summed)
            grad_t = grad_t + side_in[g, j].astype(F32) * (jnp.exp(far_top - top) / summed)
            grad_own = grad_t.T.astype(BF16)
            for xx in range(X):
                dqrow[g, j, :, pl.ds(xx * hd, hd)] = grad_own[xx * rows : (xx + 1) * rows]

        spread(g, j, inner)
        if j == 0:
            qt_sends(g, inner)

    def joined(g, j):
        arrived(dqg.at[g, pl.ds(0, rows)], xs_r + ZS * g + j)

    def block_of(g, j):
        return dqg.at[g, pl.ds(j * X * rows, X * rows)]

    def hand(g, j):
        @pl.when(inner)
        def _():
            joined(g, j)

        push(block_of(g, j), block_of(g, swap[j]), mate, g_r + ZS * g + swap[j], inner)
        if j == 1:
            push(
                dqrow.at[g, 1, :, lanes_of(x_off)], dqrow.at[g, 0, :, lanes_of(x_off)], mate,
                row_r + g, inner,
            )

    def dkv():
        pairs = [(g, j) for g in range(groups) for j in range(ZS)]

        def stacked(e, i):
            rows_in = [stat[e, slots_z[j], g, i : i + 1] for g, j in pairs]
            return jnp.concatenate(rows_in, axis=0)

        tops = [stacked(e, 0) for e in range(ZS)]
        top = functools.reduce(jnp.maximum, tops)
        scaled = [jnp.exp(m - top) for m in tops]
        summed = sum(f * stacked(e, 1) for e, f in enumerate(scaled))
        ratios = (scaled[0] / summed).T
        for n in range(0, len(pairs), 2):
            held = []
            for i, buf in enumerate((qs, dos)):
                pieces = [
                    (buf[g, j].astype(F32) * ratios[:, n + k : n + k + 1]).astype(BF16)
                    for k, (g, j) in enumerate(pairs[n : n + 2])
                ]
                held.append(jnp.concatenate(pieces, axis=0))
            span = pl.ds(n * gcols, 2 * gcols)
            for i, left in enumerate((dsbuf, pbuf)):
                piece = jnp.dot(left[:, span], held[i], preferred_element_type=F32)
                ksum[i] = piece if n == 0 else ksum[i] + piece

    kvx_r, kvt_r = take("recv", 8), take("recv", ts)
    quarter = src // 4
    stores = []

    def kvx(first, last, when):
        for n in range(first, last):
            piece = pl.ds(n % 4 * quarter, quarter)
            push(kv_out.at[n // 4, piece], kv_in.at[n // 4, piece], xpeer, kvx_r + n, when)

    def part_rows(t):
        return pl.ds(pl.multiple_of(t * part, part), part)

    def kv_finish(when):
        @pl.when(when)
        def _():
            for n in range(8):
                arrived(kv_in.at[0, pl.ds(0, quarter)], kvx_r + n)
            for i in range(2):
                kv_tp[i] = (ksum[i, :src] + kv_in[i].astype(F32)).astype(BF16)

        for e in range(1, ts):
            push(
                kv_tp.at[:, part_rows(tps[e])], kv_raw.at[:, :, head_col], dev(z, x, tps[e]),
                kvt_r + e, when,
            )

    res_r = take("recv", groups * X * ts)
    order = [(xr, e) for xr in (1, 0) for e in (3, 2, 1, 0)]

    def res_push(g, xr, e, when=None):
        k = xr * ts + e
        at = pl.ds(pl.multiple_of(tp * width + x * half + g * hd, hd), hd)
        if k:
            push(
                res_out.at[g, k], weight_raw.at[:, at], dev(z, (x, x_off)[xr], tps[e]),
                res_r + g * X * ts + k, when,
            )
        else:
            stores.append(fetch(res_out.at[g, 0], weight_raw.at[:, at]))

    def project(g):
        for xr in (1, 0):
            block = nall[pl.ds(xr * ts, ts)].reshape(ts * feat, ZS * X * rows)
            result = jnp.dot(block, dqg[g], preferred_element_type=F32).astype(BF16)
            for e in range(ts):
                res_out[g, xr * ts + e] = result[e * feat : (e + 1) * feat]

    def ready(g):
        @pl.when(edge)
        def _():
            for j in (2, 3, 1, 0):
                arrived(block_of(g, j), g_r + ZS * g + j)

    def own_rows(g):
        @pl.when(edge)
        def _():
            dqrow[g, 0, :, lanes_of(x)] = dqg[g, rows_of(0, x)]
            arrived(dqrow.at[g, 0, :, pl.ds(0, hd)], row_r + g)

        qt_sends(g, edge)

    def qt_pass(g):
        arrived(qt.at[2, g], qt_r + groups * 2 + g)
        push(qt.at[2, g], qt.at[3, g], sib_peer, qt_r + groups * 3 + g)

    def rows_part(e, g):
        left = dqrow[g, 0] if e == 0 else qt[e, g]
        total = 0.0
        for xx in range(X):
            w_cols = wbuf[e, :, pl.ds(head_of(g, xx) * hd, hd)]
            total = total + lax.dot_general(
                left[:, xx * hd : (xx + 1) * hd], w_cols, NT, preferred_element_type=F32
            )
        return total

    relay(0, 1, 3, oin)
    relay(0, 2, 2, mate)
    for g in range(1, groups):
        gather(qs, q_r, g, 0, 2, oin, inner)
        gather(dos, d_r, g, 0, 2, oin, inner)
    arrived(kbuf.at[pl.ds(src, src)], k_r)
    ktr[:, src:] = kbuf[src:].T
    peak = scores_of(0, 0)
    arrived(vbuf.at[pl.ds(src, src)], v_r)
    relay(1, 1, 3, oin)
    grads_of(0, 0, peak)
    share(0, 0)
    relay(0, 3, 3, mate)
    for j in range(1, ZS):
        arrived(delta.at[j], delta_r + j)
    gathered(0, 1)
    process(0, 1)
    for xr in range(X):
        n_send(z_oin, far, xr)
        n_send(z_oout, far, xr)
        n_send(z_mate, 1, xr)
    n_send(z, 0, 1)
    relay(1, 2, 2, mate)
    gathered(0, 2)
    process(0, 2)
    gathered(0, 3)
    process(0, 3)
    side_sum(0, 0)
    side_sum(0, 1)
    relay(1, 3, 3, mate)
    gathered(1, 1)
    side_sum(0, 2)
    for slot in range(ZS):
        for xr in range(X):
            if slot or xr:
                arrived(nall.at[0, :, pl.ds(0, rows)], n_r + X * slot + xr)
    n_pass(0, ts, xpeer)
    n_pass(0, 2, y_peer)
    n_pass(0, 1, sib_peer)
    process(1, 0)
    process(1, 1)
    side_sum(0, 3)
    gathered(1, 2)
    process(1, 2)
    n_relay(edge)
    gathered(1, 3)
    process(1, 3)
    @pl.when(inner)
    def _():
        for j in range(ZS):
            stats_came(0, j)

    reduce_rows(0, 2)
    reduce_rows(0, 3)
    hand(0, 2)
    n_relay(inner)
    reduce_rows(0, 0)
    hand(0, 3)
    side_sum(1, 0)
    side_sum(1, 1)
    reduce_rows(0, 1)
    hand(0, 0)
    side_sum(1, 2)
    hand(0, 1)
    side_sum(1, 3)
    arrived(nall.at[0], n_in + 2)
    n_pass(2, 3, sib_peer)
    arrived(nall.at[0], n_in + ts + 2)
    n_pass(ts + 2, ts + 3, sib_peer)
    @pl.when(edge)
    def _():
        for g in range(groups):
            for e in range(1, ZS):
                for j in range(ZS):
                    arrived(stat.at[0, 0, 0], stat_at(g, e, j))

    @pl.when(inner)
    def _():
        for j in range(ZS):
            stats_came(1, j)

    reduce_rows(1, 2)
    reduce_rows(1, 3)
    @pl.when(inner)
    def _():
        for i in (1, 3, ts + 1, ts + 3):
            arrived(nall.at[0], n_in + i)

        project(0)

    for e in (3, 2):
        res_push(0, 1, e, inner)
    dkv()
    kv_out[...] = ksum[:, src:].astype(BF16)
    kvx(0, 8, edge)
    hand(1, 2)
    reduce_rows(1, 0)
    hand(1, 3)
    kvx(0, 1, inner)
    for e in (3, 2, 1):
        res_push(0, 0, e, inner)
    @pl.when(edge)
    def _():
        for i in (1, 3, ts + 1, ts + 3):
            arrived(nall.at[0], n_in + i)

    ready(0)
    @pl.when(edge)
    def _():
        project(0)

    for xr in (1, 0):
        for e in (3, 2, 1, 0):
            if xr or e:
                res_push(0, xr, e, edge)
    res_push(0, 0, 0)
    own_rows(0)
    hand(1, 0)
    reduce_rows(1, 1)
    kvx(1, 8, inner)
    hand(1, 1)
    for e in (1, 0):
        res_push(0, 1, e, inner)
    qt_pass(0)
    ready(1)
    project(1)
    for xr in (1, 0):
        for e in (3, 2, 1, 0):
            res_push(1, xr, e)
    own_rows(1)
    kv_finish(edge)
    kv_finish(inner)
    stores.append(fetch(kv_tp.at[:, part_rows(tp)], kv_raw.at[:, :, head_col]))
    for copy in w_loads:
        copy.wait()
    rows_sum = rows_part(0, 0) + rows_part(0, 1) + rows_part(2, 0)
    for e in (1, 3):
        arrived(qt.at[e, 0], qt_r + groups * e)
        rows_sum = rows_sum + rows_part(e, 0)
    qt_pass(1)
    rows_sum = rows_sum + rows_part(2, 1)
    for e in (1, 3):
        arrived(qt.at[e, 1], qt_r + groups * e + 1)
        rows_sum = rows_sum + rows_part(e, 1)
    rows_out[...] = rows_sum.astype(BF16)
    stores.append(fetch(rows_out, rows_raw))
    for e in range(1, ts):
        arrived(kv_tp.at[:, pl.ds(0, part)], kvt_r + e)
    for g in range(groups):
        for xr, e in order[:-1]:
            arrived(res_out.at[g, 0], res_r + g * X * ts + xr * ts + e)
    for copy in stores:
        copy.wait()
    for copy, when in pending:
        if when is None:
            copy.wait_send()
        else:
            pl.when(when)(copy.wait_send)


def widen_kernel(
    pieces, rows_raw, weight_raw, kv_raw, grad_rows, grad_weight, grad_keys, grad_values,
    rows_in, weight_in, kv_in, weight_out, kv_out, in_sem, out_sem,
):
    step = weight_raw.shape[0] // pieces
    outs = []

    def start(source, dest, sem):
        copy = pltpu.make_async_copy(source, dest, sem)
        copy.start()
        return copy

    spans = [pl.ds(i * step, step) for i in range(pieces)]
    weight_loads = [
        start(weight_raw.at[span], weight_in.at[span], in_sem.at[3 + i])
        for i, span in enumerate(spans)
    ]
    kv_loads = [start(kv_raw.at[i], kv_in.at[i], in_sem.at[i]) for i in range(2)]
    rows_load = start(rows_raw, rows_in, in_sem.at[2])
    for i, span in enumerate(spans):
        weight_loads[i].wait()
        weight_out[span] = weight_in[span].astype(F32)
        outs.append(start(weight_out.at[span], grad_weight.at[span], out_sem.at[3 + i]))
    for i, out in enumerate((grad_keys, grad_values)):
        kv_loads[i].wait()
        kv_out[i] = kv_in[i].astype(F32)
        outs.append(start(kv_out.at[i], out, out_sem.at[i]))
    rows_load.wait()
    outs.append(start(rows_in, grad_rows, out_sem.at[2]))
    for copy in outs:
        copy.wait()


def fused(target, gain, w_query, queries, keys, values, attn_out, grad_out):
    ts = lax.axis_size("tp")
    rows, width = queries.shape
    src = keys.shape[0]
    heads = width // HEAD_DIM
    hd = HEAD_DIM
    groups, gcols = heads // X, X * rows
    feats = target.shape[1]
    feat = feats // (ZS * X)
    part = src // ts
    vmem, hbm = pl.BlockSpec(memory_space=pltpu.VMEM), pl.BlockSpec(memory_space=pl.ANY)
    part_shape = pltpu.VMEM((groups, ZS, hd, gcols), BF16)
    raw = pl.pallas_call(
        functools.partial(fused_kernel, ts, heads),
        out_shape=(
            jax.ShapeDtypeStruct((rows, feats), BF16),
            jax.ShapeDtypeStruct((feat, width * ts), BF16),
            jax.ShapeDtypeStruct((2, part, keys.shape[1]), BF16),
        ),
        in_specs=[vmem, vmem, hbm, hbm, hbm, hbm, hbm, hbm],
        out_specs=(hbm,) * 3,
        scratch_shapes=[
            pltpu.VMEM((groups, ZS, gcols, hd), BF16),
            pltpu.VMEM((groups, ZS, gcols, hd), BF16),
            pltpu.VMEM((groups, gcols, hd), BF16),
            pltpu.VMEM((X * src, hd), BF16),
            pltpu.VMEM((X * src, hd), BF16),
            pltpu.VMEM((hd, X * src), BF16),
            pltpu.VMEM((ZS, groups, 1, gcols), F32),
            pltpu.VMEM((X * src, gcols), F32),
            pltpu.VMEM((X * src, groups * ZS * gcols), BF16),
            pltpu.VMEM((X * src, groups * ZS * gcols), BF16),
            part_shape, part_shape, part_shape, part_shape,
            pltpu.VMEM((ZS, ZS, groups, 2, gcols), F32),
            pltpu.VMEM((2, X * src, hd), F32),
            pltpu.VMEM((2, src, hd), BF16),
            pltpu.VMEM((2, src, hd), BF16),
            pltpu.VMEM((2, src, hd), BF16),
            pltpu.VMEM((ts, rows, 128), F32),
            pltpu.VMEM((feats, rows), BF16),
            pltpu.VMEM((X * ts, feat, ZS * X * rows), BF16),
            pltpu.VMEM((groups, ZS, rows, X * hd), BF16),
            pltpu.VMEM((ts, groups, rows, X * hd), BF16),
            pltpu.VMEM((groups, ZS * X * rows, hd), BF16),
            pltpu.VMEM((ts, feats, width), BF16),
            pltpu.VMEM((groups, X * ts, feat, hd), BF16),
            pltpu.VMEM((rows, feats), BF16),
            pltpu.SemaphoreType.DMA((240,)),
            pltpu.SemaphoreType.DMA((190,)),
            pltpu.SemaphoreType.DMA((8 + 3 * heads + ts,)),
        ],
        compiler_params=pltpu.CompilerParams(
            collective_id=0, has_side_effects=True, vmem_limit_bytes=60 * 2**20
        ),
    )(target, gain.reshape(1, feats), w_query, queries, keys, values, attn_out, grad_out)
    return pl.pallas_call(
        functools.partial(widen_kernel, PIECES),
        out_shape=(
            jax.ShapeDtypeStruct((rows, feats), BF16),
            jax.ShapeDtypeStruct((feat, width * ts), F32),
            jax.ShapeDtypeStruct((part, keys.shape[1]), F32),
            jax.ShapeDtypeStruct((part, keys.shape[1]), F32),
        ),
        in_specs=[hbm] * 3,
        out_specs=(hbm,) * 4,
        scratch_shapes=[
            pltpu.VMEM((rows, feats), BF16),
            pltpu.VMEM((feat, width * ts), BF16),
            pltpu.VMEM((2, part, keys.shape[1]), BF16),
            pltpu.VMEM((feat, width * ts), F32),
            pltpu.VMEM((2, part, keys.shape[1]), F32),
            pltpu.SemaphoreType.DMA((3 + PIECES,)),
            pltpu.SemaphoreType.DMA((3 + PIECES,)),
        ],
    )(*raw)


def fits(mesh):
    sp, tp = mesh.shape["sp"], mesh.shape["tp"]
    feat = WIDTH // (sp * tp)
    heads = HEADS // tp
    return tp == KV_HEADS and sp == ZS * X and feat % 128 == 0 and heads == 2 * X


def solution(mesh):
    return jax.shard_map(
        fused if fits(mesh) else local,
        mesh=mesh,
        in_specs=(
            P("sp", "tp"),
            P("tp"),
            P("tp", None),
            P("sp", "tp"),
            P("sp", None),
            P("sp", None),
            P("sp", "tp"),
            P("sp", "tp"),
        ),
        out_specs=(
            P("sp", "tp"),
            P(("tp", "sp"), None),
            P(("sp", "tp"), None),
            P(("sp", "tp"), None),
        ),
        check_vma=False,
    )
```

time: 105 us -> 94.6 us (0.901); the launches traced: 104 us -> 94.5 us
  local copies, waits for them, and re-layouts: 6.46 us -> 0 us
  Pallas kernels: 96.4 us -> 93.7 us
    unnamed x8 -> x0, local copies, waits for them, and re-layouts: 6.46 us -> none
    pallas_call x1, Pallas kernels: 96.4 us -> 90.8 us  [fused(): pl.pallas_call(functools.partial(fused_kernel, ts, heads), out_shape=(jax...]
    pallas_call x0 -> x1, Pallas kernels: none -> 2.85 us  [fused(): pl.pallas_call(functools.partial(widen_kernel, PIECES), out_shape=(jax.Sh...]
where the time goes in v2:
time: 94.6 us; the launch traced here: 94.5 us
  Pallas kernels  93.7 us (99%)
    pallas_call x1, Pallas kernels, fused(): pl.pallas_call(functools.partial(fused_kernel, ts, heads), out_shape=(jax...  90.8 us
    pallas_call x1, Pallas kernels, fused(): pl.pallas_call(functools.partial(widen_kernel, PIECES), out_shape=(jax.Sh...  2.85 us

profile of v2, /device:TPU:1, one launch (start us, length us, event | category | flops | bytes accessed | tf_op | source)
XLA Modules:
  0.0 94.5 jit_solution(10933706599302427607)
XLA Ops:
  0.6 90.8 %shard_map.111 = (bf16[128,1024]{1,0:T(8,128)(2,1)}, bf16[128,4096]{1,0:T(8,128)(2,1)}, bf16[2,128,1024]{2,1,0:T(8,128)(2,1)}) custom-call(bf16[128,1024]{1,0:T(8,128)(2,1)} %target.1, f32[1,1024]{1,0:T(1,128)} %bitcast.1, bf16[1024,4096]{1,0:T(8,128)(2,1)} %w_query.1, bf16[128,1024]{1,0:T(8,128)(2,1)} %queries.1, bf16[512,1024]{1,0:T(8,128)(2,1)} %keys.1, ...), custom_call_target="tpu_custom_call" | custom-call | tf_op jit(solution)/shard_map/pallas_call | solution.py:782
  91.5 2.8 %shard_map.112 = (bf16[128,1024]{1,0:T(8,128)(2,1)}, f32[128,4096]{1,0:T(8,128)}, f32[128,1024]{1,0:T(8,128)}, f32[128,1024]{1,0:T(8,128)}) custom-call(bf16[128,1024]{1,0:T(8,128)(2,1)} %get-tuple-element.7.rows_raw, bf16[128,4096]{1,0:T(8,128)(2,1)} %get-tuple-element.8.weight_raw, bf16[2,128,1024]{2,1,0:T(8,128)(2,1)} %get-tuple-element.9.kv_raw), custom_call_target="tpu_custom_call" | custom-call | tf_op jit(solution)/shard_map/pallas_call | solution.py:825

commit v3 on v2

--- a/solution.py
+++ b/solution.py
@@ -203,7 +203,6 @@
     mate, oin, oout = (dev(a, x, tp) for a in (z_mate, z_oin, z_oout))
     xpeer, y_peer, sib_peer = dev(z, x_off, tp), dev(z, x, tps[2]), dev(z, x, sib)
     counts = {"send": 0, "recv": 0, "local": 0}
-    pending = []
 
     def take(kind, n=1):
         at = counts[kind]
@@ -216,39 +215,57 @@
             device_id=device, device_id_type=MESH,
         )
 
+    bins = []
+    small = {1: take("send"), groups: take("send")}
+
+    def planned(source, dest, device, ri, when):
+        size = math.prod(source.shape) * jnp.dtype(source.dtype).itemsize // (2 * width)
+        if source.dtype == F32 and source.shape[0] != rows:
+            return copy_of(source, dest, device, small[math.prod(source.shape[:-2])], ri)
+        for entry in bins:
+            if entry["when"] is when and entry["size"] + size <= wbuf.shape[1]:
+                break
+        else:
+            entry = {"when": when, "size": 0, "sem": take("send")}
+            bins.append(entry)
+        entry["size"] += size
+        return copy_of(source, dest, device, entry["sem"], ri)
+
     def push(source, dest, device, ri, when=None):
-        copy = copy_of(source, dest, device, take("send"), ri)
+        copy = planned(source, dest, device, ri, when)
         if when is None:
             copy.start()
         else:
             pl.when(when)(copy.start)
-        pending.append((copy, when))
 
     def arrived(view, ri):
         copy_of(view, view, xpeer, 0, ri).wait_recv()
 
-    def fetch(source, dest):
-        copy = pltpu.make_async_copy(source, dest, local_sem.at[take("local")])
+    def fetch(source, dest, sem=None):
+        sem = take("local") if sem is None else sem
+        copy = pltpu.make_async_copy(source, dest, local_sem.at[sem])
         copy.start()
         return copy
 
+    def loaded(view, sem):
+        pltpu.make_async_copy(view, view, local_sem.at[sem]).wait()
+
     def head_of(g, xx):
         return xx * groups + g
 
     head_col = pl.ds(pl.multiple_of(tp * hd, hd), hd)
-    loads = {"q": [], "d": [], "o": []}
-    for name, ref, buf in (("q", queries, qs), ("d", grad_out, dos), ("o", attn_out, outs)):
+    q_l, d_l, o_l, w_l = (take("local") for _ in range(4))
+    for sem, ref, buf in ((q_l, queries, qs), (d_l, grad_out, dos), (o_l, attn_out, outs)):
         for g in range(groups):
             for xx in range(X):
                 view = buf.at[g] if buf is outs else buf.at[g, 0]
                 view = view.at[pl.ds(xx * rows, rows)]
-                loads[name].append(fetch(ref.at[:, pl.ds(head_of(g, xx) * hd, hd)], view))
+                fetch(ref.at[:, pl.ds(head_of(g, xx) * hd, hd)], view, sem)
     k_load = fetch(keys.at[:, head_col], kbuf.at[pl.ds(0, src)])
     v_load = fetch(values.at[:, head_col], vbuf.at[pl.ds(0, src)])
-    w_loads = [
-        fetch(w_query.at[:, pl.ds(pl.multiple_of(t * width, width), width)], wbuf.at[e])
-        for e, t in enumerate(tps)
-    ]
+    for e, t in enumerate(tps):
+        w_cols = pl.ds(pl.multiple_of(t * width, width), width)
+        fetch(w_query.at[:, w_cols], wbuf.at[e], w_l)
 
     barrier = pltpu.get_barrier_semaphore()
     peers = [dev(a, x, tp) for a in slots_z[1:]] + [dev(a, x_off, tp) for a in slots_z]
@@ -258,27 +275,28 @@
 
     wide = target[...].astype(F32)
     sq[0] = jnp.broadcast_to(jnp.sum(wide * wide, axis=1, keepdims=True), (rows, 128))
-    for copy in loads["d"] + loads["o"]:
-        copy.wait()
+    loaded(dos.at[pl.ds(0, groups), 0], d_l)
+    loaded(outs, o_l)
     for g in range(groups):
         dot = jnp.sum(dos[g, 0].astype(F32) * outs[g].astype(F32), axis=1, keepdims=True)
         delta[0, g] = jnp.broadcast_to(dot, (gcols, 128)).T[:1]
-    for copy in [*loads["q"], k_load, v_load]:
-        copy.wait()
+    loaded(qs.at[pl.ds(0, groups), 0], q_l)
+    k_load.wait()
+    v_load.wait()
     pl.semaphore_wait(barrier, len(peers))
 
     q_r, d_r = take("recv", ZS * groups), take("recv", ZS * groups)
-    delta_r, sq_r = take("recv", ZS), take("recv", ZS)
+    delta_r, sq_r = take("recv"), take("recv")
     k_r, v_r = take("recv"), take("recv")
 
     def gather(buf, base, g, a, b, device, when=None):
         push(buf.at[g, a], buf.at[g, b], device, base + ZS * g + b, when)
 
-    push(delta.at[0], delta.at[1], mate, delta_r + 1)
-    push(delta.at[0], delta.at[far], oin, delta_r + far)
-    push(delta.at[0], delta.at[far], oout, delta_r + far)
+    push(delta.at[0], delta.at[1], mate, delta_r)
+    push(delta.at[0], delta.at[far], oin, delta_r)
+    push(delta.at[0], delta.at[far], oout, delta_r)
     for e in range(1, ts):
-        push(sq.at[0], sq.at[e], dev(z, x, tps[e]), sq_r + e)
+        push(sq.at[0], sq.at[e], dev(z, x, tps[e]), sq_r)
     gather(qs, q_r, 0, 0, 1, mate)
     gather(qs, q_r, 0, 0, 2, oin, inner)
     push(kbuf.at[pl.ds(0, src)], kbuf.at[pl.ds(src, src)], xpeer, k_r)
@@ -290,8 +308,7 @@
         gather(dos, d_r, g, 0, 1, mate)
 
     ktr[:, :src] = kbuf[:src].T
-    for e in range(1, ts):
-        arrived(sq.at[e], sq_r + e)
+    arrived(sq.at[pl.ds(1, ts - 1)], sq_r)
     total = sq[0]
     for e in range(1, ts):
         total = total + sq[e]
@@ -305,23 +322,23 @@
     def lanes(slot, xx):
         return pl.ds(pl.multiple_of((slot * X + xx) * rows, rows), rows)
 
-    n_r = take("recv", ZS * X)
-    n_in = take("recv", X * ts)
+    n_r, n_sib = take("recv"), take("recv")
+    n_in = {ts: take("recv"), 2: take("recv"), ts + 2: take("recv")}
 
     def n_send(zz, slot, xr):
         xx = (x, x_off)[xr]
         push(
             ntr.at[feature_rows(zz, xx)], nall.at[0, :, lanes(slot, x)], dev(zz, xx, tp),
-            n_r + X * slot + xr,
+            n_r,
         )
 
     def n_pass(i, to, device, when=None):
-        push(nall.at[i], nall.at[to], device, n_in + to, when)
+        push(nall.at[i], nall.at[to], device, n_in.get(to, n_sib), when)
 
     def n_relay(when):
         @pl.when(when)
         def _():
-            arrived(nall.at[0], n_in + ts)
+            arrived(nall.at[0], n_in[ts])
 
         n_pass(ts, ts + 2, y_peer, when)
         n_pass(ts, ts + 1, sib_peer, when)
@@ -330,16 +347,12 @@
 
     def relay(g, a, b, device):
         for buf, base in ((qs, q_r), (dos, d_r)):
-            copy = copy_of(
-                buf.at[g, a], buf.at[g, b], device, take("send"), base + ZS * g + b
-            )
+            copy = planned(buf.at[g, a], buf.at[g, b], device, base + ZS * g + b, inner)
 
             @pl.when(inner)
             def _():
                 arrived(buf.at[g, a], base + ZS * g + a)
                 copy.start()
-
-            pending.append((copy, inner))
 
     def gathered(g, a):
         @pl.when(edge)
@@ -375,16 +388,17 @@
         stat[0, slots_z[j], g, 1:2] = total
         qpart[g, j] = jnp.dot(ktr[...], dsbuf[:, lane_span], preferred_element_type=F32).astype(BF16)
 
-    stat_r = take("recv", groups * ZS * ZS)
+    stat_r = take("recv", groups * (ZS + 1))
     part_r, side_r = take("recv", groups * ZS), take("recv", groups * ZS)
 
-    def stat_at(g, e, j):
-        return stat_r + ZS * ZS * g + ZS * e + j
+    def mate_stat(g, j):
+        return stat_r + (ZS + 1) * g + j
 
     def share(g, j):
         zt = slots_z[j]
-        for e, device in ((far, oin), (far, oout), (1, mate)):
-            push(stat.at[0, zt, g], stat.at[e, zt, g], device, stat_at(g, e, j))
+        for device in (oin, oout):
+            push(stat.at[0, zt, g], stat.at[far, zt, g], device, mate_stat(g, ZS))
+        push(stat.at[0, zt, g], stat.at[1, zt, g], mate, mate_stat(g, j))
         to = swap[j]
         push(qpart.at[g, j], part_in.at[g, to], mate, part_r + ZS * g + to, edge)
 
@@ -400,15 +414,13 @@
         summed = sum(f * stat[e, zt, g, 1:2] for e, f in zip(sources, scaled))
         return top, scaled, summed
 
-    def stats_came(g, j):
-        there = (j + 2) % ZS
-        for e, k in ((2, there), (3, there if there > 1 else swap[there])):
-            arrived(stat.at[0, 0, 0], stat_at(g, e, k))
+    def stats_came(g):
+        arrived(stat.at[pl.ds(2, 2), pl.ds(0, ZS), g], mate_stat(g, ZS))
 
     def side_sum(g, j):
         @pl.when(inner)
         def _():
-            arrived(stat.at[0, 0, 0], stat_at(g, 1, swap[j]))
+            arrived(stat.at[0, 0, 0], mate_stat(g, swap[j]))
             arrived(part_in.at[g, j], part_r + ZS * g + j)
             _, (f_own, f_mate), _ = weights_of(g, j, (0, 1))
             near_part = qpart[g, j].astype(F32) * f_own + part_in[g, j].astype(F32) * f_mate
@@ -417,8 +429,8 @@
         to = (j + 2) % ZS
         push(side_out.at[g, j], side_in.at[g, to], oin, side_r + ZS * g + to, inner)
 
-    row_r, xs_r, g_r = (take("recv", groups * ZS) for _ in range(3))
-    qt_r = take("recv", ts * groups)
+    row_r, g_r, xs_r = take("recv", groups), take("recv", groups), take("recv", groups * ZS)
+    qt_r, qs_r = take("recv", groups), take("recv", groups)
 
     def rows_of(slot, xx):
         return pl.ds(pl.multiple_of((slot * X + xx) * rows, rows), rows)
@@ -437,8 +449,8 @@
             dqg[g, rows_of(j, x)] = dqrow[g, j, :, lanes_of(x)]
 
     def qt_sends(g, when):
-        push(dqrow.at[g, 0], qt.at[2, g], y_peer, qt_r + groups * 2 + g, when)
-        push(dqrow.at[g, 0], qt.at[1, g], sib_peer, qt_r + groups + g, when)
+        push(dqrow.at[g, 0], qt.at[2, g], y_peer, qt_r + g, when)
+        push(dqrow.at[g, 0], qt.at[1, g], sib_peer, qs_r + g, when)
 
     def reduce_rows(g, j):
         @pl.when(inner)
@@ -467,11 +479,19 @@
         def _():
             joined(g, j)
 
-        push(block_of(g, j), block_of(g, swap[j]), mate, g_r + ZS * g + swap[j], inner)
-        if j == 1:
+        push(block_of(g, j), block_of(g, swap[j]), mate, g_r + g, inner)
+
+    def hand_rows(g):
+        push(
+            dqrow.at[g, 1, :, lanes_of(x_off)], dqrow.at[g, 0, :, lanes_of(x_off)], mate,
+            row_r + g, inner,
+        )
+
+    def hand_direct(g):
+        for xx in (x_off, x):
             push(
-                dqrow.at[g, 1, :, lanes_of(x_off)], dqrow.at[g, 0, :, lanes_of(x_off)], mate,
-                row_r + g, inner,
+                dqrow.at[g, 1, :, lanes_of(xx)], dqg.at[g, rows_of(0, x)], dev(z_mate, xx, tp),
+                g_r + g, inner,
             )
 
     def dkv():
@@ -499,14 +519,14 @@
                 piece = jnp.dot(left[:, span], held[i], preferred_element_type=F32)
                 ksum[i] = piece if n == 0 else ksum[i] + piece
 
-    kvx_r, kvt_r = take("recv", 8), take("recv", ts)
+    kvx_r, kvt_r = take("recv"), take("recv")
     quarter = src // 4
     stores = []
 
     def kvx(first, last, when):
         for n in range(first, last):
             piece = pl.ds(n % 4 * quarter, quarter)
-            push(kv_out.at[n // 4, piece], kv_in.at[n // 4, piece], xpeer, kvx_r + n, when)
+            push(kv_out.at[n // 4, piece], kv_in.at[n // 4, piece], xpeer, kvx_r, when)
 
     def part_rows(t):
         return pl.ds(pl.multiple_of(t * part, part), part)
@@ -514,19 +534,17 @@
     def kv_finish(when):
         @pl.when(when)
         def _():
-            for n in range(8):
-                arrived(kv_in.at[0, pl.ds(0, quarter)], kvx_r + n)
+            arrived(kv_in, kvx_r)
             for i in range(2):
                 kv_tp[i] = (ksum[i, :src] + kv_in[i].astype(F32)).astype(BF16)
 
         for e in range(1, ts):
             push(
                 kv_tp.at[:, part_rows(tps[e])], kv_raw.at[:, :, head_col], dev(z, x, tps[e]),
-                kvt_r + e, when,
+                kvt_r, when,
             )
 
-    res_r = take("recv", groups * X * ts)
-    order = [(xr, e) for xr in (1, 0) for e in (3, 2, 1, 0)]
+    res_r = take("recv")
 
     def res_push(g, xr, e, when=None):
         k = xr * ts + e
@@ -534,7 +552,7 @@
         if k:
             push(
                 res_out.at[g, k], weight_raw.at[:, at], dev(z, (x, x_off)[xr], tps[e]),
-                res_r + g * X * ts + k, when,
+                res_r, when,
             )
         else:
             stores.append(fetch(res_out.at[g, 0], weight_raw.at[:, at]))
@@ -549,8 +567,7 @@
     def ready(g):
         @pl.when(edge)
         def _():
-            for j in (2, 3, 1, 0):
-                arrived(block_of(g, j), g_r + ZS * g + j)
+            arrived(dqg.at[g], g_r + g)
 
     def own_rows(g):
         @pl.when(edge)
@@ -561,8 +578,8 @@
         qt_sends(g, edge)
 
     def qt_pass(g):
-        arrived(qt.at[2, g], qt_r + groups * 2 + g)
-        push(qt.at[2, g], qt.at[3, g], sib_peer, qt_r + groups * 3 + g)
+        arrived(qt.at[2, g], qt_r + g)
+        push(qt.at[2, g], qt.at[3, g], sib_peer, qs_r + g)
 
     def rows_part(e, g):
         left = dqrow[g, 0] if e == 0 else qt[e, g]
@@ -587,8 +604,7 @@
     grads_of(0, 0, peak)
     share(0, 0)
     relay(0, 3, 3, mate)
-    for j in range(1, ZS):
-        arrived(delta.at[j], delta_r + j)
+    arrived(delta.at[pl.ds(1, ZS - 1)], delta_r)
     gathered(0, 1)
     process(0, 1)
     for xr in range(X):
@@ -606,10 +622,7 @@
     relay(1, 3, 3, mate)
     gathered(1, 1)
     side_sum(0, 2)
-    for slot in range(ZS):
-        for xr in range(X):
-            if slot or xr:
-                arrived(nall.at[0, :, pl.ds(0, rows)], n_r + X * slot + xr)
+    arrived(nall.at[0, :, pl.ds(0, (ZS * X - 1) * rows)], n_r)
     n_pass(0, ts, xpeer)
     n_pass(0, 2, y_peer)
     n_pass(0, 1, sib_peer)
@@ -623,8 +636,7 @@
     process(1, 3)
     @pl.when(inner)
     def _():
-        for j in range(ZS):
-            stats_came(0, j)
+        stats_came(0)
 
     reduce_rows(0, 2)
     reduce_rows(0, 3)
@@ -638,29 +650,28 @@
     hand(0, 0)
     side_sum(1, 2)
     hand(0, 1)
+    hand_rows(0)
     side_sum(1, 3)
-    arrived(nall.at[0], n_in + 2)
+    arrived(nall.at[0], n_in[2])
     n_pass(2, 3, sib_peer)
-    arrived(nall.at[0], n_in + ts + 2)
+    arrived(nall.at[0], n_in[ts + 2])
     n_pass(ts + 2, ts + 3, sib_peer)
     @pl.when(edge)
     def _():
         for g in range(groups):
-            for e in range(1, ZS):
-                for j in range(ZS):
-                    arrived(stat.at[0, 0, 0], stat_at(g, e, j))
+            for j in range(ZS):
+                arrived(stat.at[0, 0, 0], mate_stat(g, j))
+            stats_came(g)
 
     @pl.when(inner)
     def _():
-        for j in range(ZS):
-            stats_came(1, j)
+        stats_came(1)
 
     reduce_rows(1, 2)
     reduce_rows(1, 3)
     @pl.when(inner)
     def _():
-        for i in (1, 3, ts + 1, ts + 3):
-            arrived(nall.at[0], n_in + i)
+        arrived(nall.at[pl.ds(0, ts)], n_sib)
 
         project(0)
 
@@ -677,8 +688,7 @@
         res_push(0, 0, e, inner)
     @pl.when(edge)
     def _():
-        for i in (1, 3, ts + 1, ts + 3):
-            arrived(nall.at[0], n_in + i)
+        arrived(nall.at[pl.ds(0, ts)], n_sib)
 
     ready(0)
     @pl.when(edge)
@@ -693,45 +703,49 @@
     own_rows(0)
     hand(1, 0)
     reduce_rows(1, 1)
+    hand_direct(1)
+    hand_rows(1)
     kvx(1, 8, inner)
-    hand(1, 1)
+
+    @pl.when(inner)
+    def _():
+        joined(1, 1)
+
     for e in (1, 0):
         res_push(0, 1, e, inner)
     qt_pass(0)
+    kv_finish(edge)
     ready(1)
+    own_rows(1)
     project(1)
     for xr in (1, 0):
         for e in (3, 2, 1, 0):
             res_push(1, xr, e)
-    own_rows(1)
-    kv_finish(edge)
     kv_finish(inner)
     stores.append(fetch(kv_tp.at[:, part_rows(tp)], kv_raw.at[:, :, head_col]))
-    for copy in w_loads:
-        copy.wait()
+    loaded(wbuf, w_l)
     rows_sum = rows_part(0, 0) + rows_part(0, 1) + rows_part(2, 0)
+    arrived(qt.at[pl.ds(0, 2), 0], qs_r)
     for e in (1, 3):
-        arrived(qt.at[e, 0], qt_r + groups * e)
         rows_sum = rows_sum + rows_part(e, 0)
     qt_pass(1)
     rows_sum = rows_sum + rows_part(2, 1)
+    arrived(qt.at[pl.ds(0, 2), 1], qs_r + 1)
     for e in (1, 3):
-        arrived(qt.at[e, 1], qt_r + groups * e + 1)
         rows_sum = rows_sum + rows_part(e, 1)
     rows_out[...] = rows_sum.astype(BF16)
     stores.append(fetch(rows_out, rows_raw))
-    for e in range(1, ts):
-        arrived(kv_tp.at[:, pl.ds(0, part)], kvt_r + e)
-    for g in range(groups):
-        for xr, e in order[:-1]:
-            arrived(res_out.at[g, 0], res_r + g * X * ts + xr * ts + e)
+    arrived(kv_raw.at[:, :, pl.ds(0, (ts - 1) * hd)], kvt_r)
+    arrived(weight_raw.at[:, pl.ds(0, groups * (X * ts - 1) * hd)], res_r)
     for copy in stores:
         copy.wait()
-    for copy, when in pending:
-        if when is None:
-            copy.wait_send()
-        else:
-            pl.when(when)(copy.wait_send)
+    for sent, sem in ((stat.at[pl.ds(0, ZS - 1)], small[1]), (delta.at[pl.ds(1, ZS - 1)], small[groups])):
+        copy_of(sent, sent, xpeer, sem, 0).wait_send()
+    for entry in bins:
+        sent = wbuf.at[0, pl.ds(0, entry["size"])]
+        wait = copy_of(sent, sent, xpeer, entry["sem"], 0).wait_send
+        wait() if entry["when"] is None else pl.when(entry["when"])(wait)
+    assert counts["send"] <= send.shape[0] and counts["recv"] <= recv.shape[0]
 
 
 def widen_kernel(
@@ -814,9 +828,9 @@
             pltpu.VMEM((ts, feats, width), BF16),
             pltpu.VMEM((groups, X * ts, feat, hd), BF16),
             pltpu.VMEM((rows, feats), BF16),
-            pltpu.SemaphoreType.DMA((240,)),
-            pltpu.SemaphoreType.DMA((190,)),
-            pltpu.SemaphoreType.DMA((8 + 3 * heads + ts,)),
+            pltpu.SemaphoreType.DMA((16,)),
+            pltpu.SemaphoreType.DMA((76,)),
+            pltpu.SemaphoreType.DMA((12,)),
         ],
         compiler_params=pltpu.CompilerParams(
             collective_id=0, has_side_effects=True, vmem_limit_bytes=60 * 2**20

time: 94.6 us -> 89 us (0.941); the launches traced: 94.5 us -> 87.6 us
  Pallas kernels: 93.7 us -> 86.8 us
    pallas_call x1, Pallas kernels: 90.8 us -> 83.9 us  [fused(): pl.pallas_call(functools.partial(fused_kernel, ts, heads), out_shape=(jax...]
where the time goes in v3:
time: 89 us; the launch traced here: 87.6 us
  Pallas kernels  86.8 us (98%)
    pallas_call x1, Pallas kernels, fused(): pl.pallas_call(functools.partial(fused_kernel, ts, heads), out_shape=(jax...  83.9 us
    pallas_call x1, Pallas kernels, fused(): pl.pallas_call(functools.partial(widen_kernel, PIECES), out_shape=(jax.Sh...  2.85 us

profile of v3, /device:TPU:1, one launch (start us, length us, event | category | flops | bytes accessed | tf_op | source)
XLA Modules:
  0.0 87.6 jit_solution(6543053651768014126)
XLA Ops:
  0.6 83.9 %shard_map.111 = (bf16[128,1024]{1,0:T(8,128)(2,1)}, bf16[128,4096]{1,0:T(8,128)(2,1)}, bf16[2,128,1024]{2,1,0:T(8,128)(2,1)}) custom-call(bf16[128,1024]{1,0:T(8,128)(2,1)} %target.1, f32[1,1024]{1,0:T(1,128)} %bitcast.1, bf16[1024,4096]{1,0:T(8,128)(2,1)} %w_query.1, bf16[128,1024]{1,0:T(8,128)(2,1)} %queries.1, bf16[512,1024]{1,0:T(8,128)(2,1)} %keys.1, ...), custom_call_target="tpu_custom_call" | custom-call | tf_op jit(solution)/shard_map/pallas_call | solution.py:796
  84.5 2.8 %shard_map.112 = (bf16[128,1024]{1,0:T(8,128)(2,1)}, f32[128,4096]{1,0:T(8,128)}, f32[128,1024]{1,0:T(8,128)}, f32[128,1024]{1,0:T(8,128)}) custom-call(bf16[128,1024]{1,0:T(8,128)(2,1)} %get-tuple-element.7.rows_raw, bf16[128,4096]{1,0:T(8,128)(2,1)} %get-tuple-element.8.weight_raw, bf16[2,128,1024]{2,1,0:T(8,128)(2,1)} %get-tuple-element.9.kv_raw), custom_call_target="tpu_custom_call" | custom-call | tf_op jit(solution)/shard_map/pallas_call | solution.py:839

commit v4 on v3

--- a/solution.py
+++ b/solution.py
@@ -166,11 +166,11 @@
 
 def fused_kernel(
     ts, heads,
-    target, gain, w_query, queries, keys, values, attn_out, grad_out,
+    target_hbm, gain_hbm, w_query, queries, keys, values, attn_out, grad_out,
     rows_raw, weight_raw, kv_raw,
     qs, dos, outs, kbuf, vbuf, ktr, delta, sbuf, pbuf, dsbuf, qpart, part_in,
     side_out, side_in, stat, ksum, kv_out, kv_in, kv_tp, sq, ntr, nall,
-    dqrow, qt, dqg, wbuf, res_out, rows_out, send, recv, local_sem,
+    dqrow, qt, dqg, wbuf, res_out, rows_out, target, gain, send, recv, local_sem,
 ):
     rows = queries.shape[0]
     src = keys.shape[0]
@@ -250,10 +250,17 @@
     def loaded(view, sem):
         pltpu.make_async_copy(view, view, local_sem.at[sem]).wait()
 
+    barrier = pltpu.get_barrier_semaphore()
+    peers = [dev(a, x, tp) for a in slots_z[1:]] + [dev(a, x_off, tp) for a in slots_z]
+    peers += [dev(z, xx, t) for xx in (x, x_off) for t in tps[1:]]
+    for peer in peers:
+        pl.semaphore_signal(barrier, inc=1, device_id=peer, device_id_type=MESH)
+
     def head_of(g, xx):
         return xx * groups + g
 
     head_col = pl.ds(pl.multiple_of(tp * hd, hd), hd)
+    t_load, gain_load = fetch(target_hbm, target), fetch(gain_hbm, gain)
     q_l, d_l, o_l, w_l = (take("local") for _ in range(4))
     for sem, ref, buf in ((q_l, queries, qs), (d_l, grad_out, dos), (o_l, attn_out, outs)):
         for g in range(groups):
@@ -267,12 +274,8 @@
         w_cols = pl.ds(pl.multiple_of(t * width, width), width)
         fetch(w_query.at[:, w_cols], wbuf.at[e], w_l)
 
-    barrier = pltpu.get_barrier_semaphore()
-    peers = [dev(a, x, tp) for a in slots_z[1:]] + [dev(a, x_off, tp) for a in slots_z]
-    peers += [dev(z, xx, t) for xx in (x, x_off) for t in tps[1:]]
-    for peer in peers:
-        pl.semaphore_signal(barrier, inc=1, device_id=peer, device_id_type=MESH)
-
+    t_load.wait()
+    gain_load.wait()
     wide = target[...].astype(F32)
     sq[0] = jnp.broadcast_to(jnp.sum(wide * wide, axis=1, keepdims=True), (rows, 128))
     loaded(dos.at[pl.ds(0, groups), 0], d_l)
@@ -667,6 +670,9 @@
     def _():
         stats_came(1)
 
+    dkv()
+    kv_out[...] = ksum[:, src:].astype(BF16)
+    kvx(0, 8, edge)
     reduce_rows(1, 2)
     reduce_rows(1, 3)
     @pl.when(inner)
@@ -677,13 +683,10 @@
 
     for e in (3, 2):
         res_push(0, 1, e, inner)
-    dkv()
-    kv_out[...] = ksum[:, src:].astype(BF16)
-    kvx(0, 8, edge)
     hand(1, 2)
     reduce_rows(1, 0)
     hand(1, 3)
-    kvx(0, 1, inner)
+    kvx(0, 3, inner)
     for e in (3, 2, 1):
         res_push(0, 0, e, inner)
     @pl.when(edge)
@@ -705,7 +708,7 @@
     reduce_rows(1, 1)
     hand_direct(1)
     hand_rows(1)
-    kvx(1, 8, inner)
+    kvx(3, 8, inner)
 
     @pl.when(inner)
     def _():
@@ -791,7 +794,7 @@
     feats = target.shape[1]
     feat = feats // (ZS * X)
     part = src // ts
-    vmem, hbm = pl.BlockSpec(memory_space=pltpu.VMEM), pl.BlockSpec(memory_space=pl.ANY)
+    hbm = pl.BlockSpec(memory_space=pl.ANY)
     part_shape = pltpu.VMEM((groups, ZS, hd, gcols), BF16)
     raw = pl.pallas_call(
         functools.partial(fused_kernel, ts, heads),
@@ -800,7 +803,7 @@
             jax.ShapeDtypeStruct((feat, width * ts), BF16),
             jax.ShapeDtypeStruct((2, part, keys.shape[1]), BF16),
         ),
-        in_specs=[vmem, vmem, hbm, hbm, hbm, hbm, hbm, hbm],
+        in_specs=[hbm] * 8,
         out_specs=(hbm,) * 3,
         scratch_shapes=[
             pltpu.VMEM((groups, ZS, gcols, hd), BF16),
@@ -828,9 +831,11 @@
             pltpu.VMEM((ts, feats, width), BF16),
             pltpu.VMEM((groups, X * ts, feat, hd), BF16),
             pltpu.VMEM((rows, feats), BF16),
+            pltpu.VMEM((rows, feats), BF16),
+            pltpu.VMEM((1, feats), F32),
             pltpu.SemaphoreType.DMA((16,)),
             pltpu.SemaphoreType.DMA((76,)),
-            pltpu.SemaphoreType.DMA((12,)),
+            pltpu.SemaphoreType.DMA((14,)),
         ],
         compiler_params=pltpu.CompilerParams(
             collective_id=0, has_side_effects=True, vmem_limit_bytes=60 * 2**20

time: 89 us -> 87.7 us (0.985); the launches traced: 87.6 us -> 87.6 us
  no operation moved by 1% of the time
where the time goes in v4:
time: 87.7 us; the launch traced here: 87.6 us
  Pallas kernels  86.8 us (99%)
    pallas_call x1, Pallas kernels, fused(): pl.pallas_call(functools.partial(fused_kernel, ts, heads), out_shape=(jax...  83.9 us
    pallas_call x1, Pallas kernels, fused(): pl.pallas_call(functools.partial(widen_kernel, PIECES), out_shape=(jax.Sh...  2.85 us

profile of v4, /device:TPU:1, one launch (start us, length us, event | category | flops | bytes accessed | tf_op | source)
XLA Modules:
  0.0 87.6 jit_solution(13411928711423968000)
XLA Ops:
  0.6 83.9 %shard_map.111 = (bf16[128,1024]{1,0:T(8,128)(2,1)}, bf16[128,4096]{1,0:T(8,128)(2,1)}, bf16[2,128,1024]{2,1,0:T(8,128)(2,1)}) custom-call(bf16[128,1024]{1,0:T(8,128)(2,1)} %target_hbm.1, f32[1,1024]{1,0:T(1,128)} %bitcast.1, bf16[1024,4096]{1,0:T(8,128)(2,1)} %w_query.1, bf16[128,1024]{1,0:T(8,128)(2,1)} %queries.1, bf16[512,1024]{1,0:T(8,128)(2,1)} %keys.1, ...), custom_call_target="tpu_custom_call" | custom-call | tf_op jit(solution)/shard_map/pallas_call | solution.py:799
  84.6 2.8 %shard_map.112 = (bf16[128,1024]{1,0:T(8,128)(2,1)}, f32[128,4096]{1,0:T(8,128)}, f32[128,1024]{1,0:T(8,128)}, f32[128,1024]{1,0:T(8,128)}) custom-call(bf16[128,1024]{1,0:T(8,128)(2,1)} %get-tuple-element.7.rows_raw, bf16[128,4096]{1,0:T(8,128)(2,1)} %get-tuple-element.8.weight_raw, bf16[2,128,1024]{2,1,0:T(8,128)(2,1)} %get-tuple-element.9.kv_raw), custom_call_target="tpu_custom_call" | custom-call | tf_op jit(solution)/shard_map/pallas_call | solution.py:844

commit v5 on v4

--- a/solution.py
+++ b/solution.py
@@ -161,7 +161,7 @@
 X = 2
 ZS = 4
 CHUNK = 512
-PIECES = 4
+PIECES = 8
 
 
 def fused_kernel(

time: 87.7 us -> 87.7 us (level)
  no operation moved by 1% of the time
where the time goes in v5:
time: 87.7 us; the launch traced here: 87.6 us
  Pallas kernels  86.8 us (99%)
    pallas_call x1, Pallas kernels, fused(): pl.pallas_call(functools.partial(fused_kernel, ts, heads), out_shape=(jax...  83.9 us
    pallas_call x1, Pallas kernels, fused(): pl.pallas_call(functools.partial(widen_kernel, PIECES), out_shape=(jax.Sh...  2.85 us

profile of v5, /device:TPU:1, one launch (start us, length us, event | category | flops | bytes accessed | tf_op | source)
XLA Modules:
  0.0 87.6 jit_solution(2333427763661513348)
XLA Ops:
  0.6 83.9 %shard_map.111 = (bf16[128,1024]{1,0:T(8,128)(2,1)}, bf16[128,4096]{1,0:T(8,128)(2,1)}, bf16[2,128,1024]{2,1,0:T(8,128)(2,1)}) custom-call(bf16[128,1024]{1,0:T(8,128)(2,1)} %target_hbm.1, f32[1,1024]{1,0:T(1,128)} %bitcast.1, bf16[1024,4096]{1,0:T(8,128)(2,1)} %w_query.1, bf16[128,1024]{1,0:T(8,128)(2,1)} %queries.1, bf16[512,1024]{1,0:T(8,128)(2,1)} %keys.1, ...), custom_call_target="tpu_custom_call" | custom-call | tf_op jit(solution)/shard_map/pallas_call | solution.py:799
  84.6 2.9 %shard_map.112 = (bf16[128,1024]{1,0:T(8,128)(2,1)}, f32[128,4096]{1,0:T(8,128)}, f32[128,1024]{1,0:T(8,128)}, f32[128,1024]{1,0:T(8,128)}) custom-call(bf16[128,1024]{1,0:T(8,128)(2,1)} %get-tuple-element.7.rows_raw, bf16[128,4096]{1,0:T(8,128)(2,1)} %get-tuple-element.8.weight_raw, bf16[2,128,1024]{2,1,0:T(8,128)(2,1)} %get-tuple-element.9.kv_raw), custom_call_target="tpu_custom_call" | custom-call | tf_op jit(solution)/shard_map/pallas_call | solution.py:844
